TPU v7x, 128 devices: a whole 4x4x4 slice. The times are simulated.
128 devices in a mesh: sp: 32 (over z, y, core), tp: 4 (over x).
Axes of the slice: x: 4, y: 4, z: 4, core: 2. Of those that a mesh axis runs over, the one named last changes fastest.
Arguments:
- tokens: bfloat16 [8192, 4096], P('sp', 'tp'), may hold values from -6 to 6
- input_norm_gain: float32 [4096], replicated, may hold values from 0.1 to 1.9
- query_weight: bfloat16 [4096, 2048], P('sp', 'tp'), may hold values from -0.09375 to 0.09375
- key_weight: bfloat16 [4096, 2048], P('sp', 'tp'), may hold values from -0.09375 to 0.09375
- value_weight: bfloat16 [4096, 2048], P('sp', 'tp'), may hold values from -0.09375 to 0.09375
- decay_first_map: bfloat16 [4096, 128], replicated, may hold values from -0.09375 to 0.09375
- decay_second_map: bfloat16 [128, 2048], P(None, 'tp'), may hold values from -0.5 to 0.5
- channel_decay_offset: float32 [2048], P('tp'), may hold values from -13 to -2
- position_decay_offset: float32 [8192], P('sp'), may hold values from -2 to 2
- extra_log_decay: float32 [8192, 32], P('sp', 'tp'), may hold values from -0.7 to 0
- rate_first_map: bfloat16 [4096, 128], replicated, may hold values from -0.09375 to 0.09375
- rate_second_map: bfloat16 [128, 2048], P(None, 'tp'), may hold values from -0.25 to 0.25
- channel_rate_offset: float32 [2048], P('tp'), may hold values from -10 to 1
- own_term_weight: float32 [2048], P('tp'), may hold values from -2 to 2
- head_norm_gain: float32 [2048], P('tp'), may hold values from 0.1 to 1.9
- starting_state: float32 [32, 64, 64], P('tp'), may hold values from -384 to 384
- outer_gate_weight: bfloat16 [4096, 2048], P('sp', 'tp'), may hold values from -0.09375 to 0.09375
- inner_gate_weight: bfloat16 [4096, 2048], P('sp', 'tp'), may hold values from -0.09375 to 0.09375
- signal_weight: bfloat16 [4096, 2048], P('sp', 'tp'), may hold values from -0.09375 to 0.09375
- convolution_taps: bfloat16 [3, 2048], P(None, 'tp'), may hold values from -3.5 to 3.5
- convolution_gain: float32 [2048], P('tp'), may hold values from 0.1 to 1.9
Outputs:
- linear_attention_output: bfloat16 [8192, 2048], P('sp', 'tp')
- out_conv: bfloat16 [8192, 2048], P('sp', 'tp')
All inputs are finite; a program needn't handle non-finite values.
Results may differ from a plain program's by a relative error of at most 0.009.
Values may be sent and summed in bfloat16 or wider, within the bound.
A program may use at most 128 MiB of HBM per device.

v0:
```python
import jax
import jax.numpy as jnp
from jax import lax
from jax.sharding import Mesh
from jax.sharding import PartitionSpec as P

BLOCK = 64
SP = ("sp_0", "sp_1", "sp_2")


DECAY_FACTOR = 0.606531
NORM_EPS = 1e-06
GROUP_EPS = 0.00064
KEY_EPS = 1e-06


def copy_for_each(value, axis):
    copies = jnp.broadcast_to(value, (lax.axis_size(axis), *value.shape))
    return lax.all_to_all(copies, axis, split_axis=0, concat_axis=0, tiled=True)


def joined_along(pieces, dim):
    pieces = jnp.moveaxis(pieces, 0, dim)
    shape = pieces.shape
    return pieces.reshape(*shape[:dim], shape[dim] * shape[dim + 1], *shape[dim + 2 :])


def gathered_copies(value, axis, dim):
    pieces = copy_for_each(value, axis)
    return joined_along(pieces, dim)


def in_one_piece(arrays, axis, dim, along):
    widths = [a.shape[along] for a in arrays]
    both = jnp.concatenate(arrays, axis=along)
    out = lax.all_gather(both, axis, axis=dim, tiled=True)
    return tuple(jnp.split(out, [sum(widths[:k]) for k in range(1, len(widths))], axis=along))


def filled_with(value, identity):
    return jax.tree.map(
        lambda a, e: jnp.broadcast_to(jnp.asarray(e, a.dtype), a.shape), value, identity
    )


def entering_2(value, axes, combine, identity):
    before = start = filled_with(value, identity)
    subtotal = value
    for axis in reversed(axes):
        length, position = (lax.axis_size(axis), lax.axis_index(axis))
        pieces = jax.tree.map(
            lambda part, kind: lax.all_gather(part.astype(kind), axis),
            subtotal,
            (jnp.bfloat16, jnp.bfloat16),
        )
        inside, subtotal = (start, start)
        for k in range(length):
            passed = k < position
            subtotal = combine(
                subtotal, jax.tree.map(lambda part, own: part[k].astype(own.dtype), pieces, value)
            )
            inside = jax.tree.map(lambda new, old: jnp.where(passed, new, old), subtotal, inside)
        before = combine(inside, before)
    return before


def from_behind(block, axis, distance):
    devices = range(lax.axis_size(axis))
    route = [(i - distance, i) for i in devices if i - distance in devices]
    return lax.ppermute(block, axis, route)


def over_copies(value, axis):
    everything = copy_for_each(value, axis)
    return jnp.sum(everything, axis=0)


def rounded(values):
    return lax.optimization_barrier(values.astype(jnp.bfloat16)).astype(jnp.float32)


def contract(spec, left, right):
    return jnp.einsum(spec, left, right, precision=lax.Precision.HIGHEST)


def fold_rows(normed):

    def accumulate(totals, pieces, offset):
        return tuple(
            (
                jnp.dot(normed, weight_piece, preferred_element_type=jnp.float32)
                for weight_piece in pieces
            )
        )

    return accumulate


def mixer_blocks(query, keyed, valued, unit_key, decay_logarithm, rate):
    sequence_length, number_heads, head_dimension = query.shape
    block_size = BLOCK
    count = sequence_length // block_size
    eye_heads = jnp.broadcast_to(
        jnp.eye(head_dimension, dtype=jnp.float32), (number_heads, head_dimension, head_dimension)
    )
    eye_block = jnp.eye(block_size, dtype=jnp.float32)
    later = jnp.arange(block_size)[:, None]
    earlier = jnp.arange(block_size)[None, :]
    strict = later > earlier
    inclusive = later >= earlier
    block_shape = (count, block_size, number_heads, head_dimension)
    query_b, keyed_b, valued_b, unit_b, decay_b, rate_b = (
        values.reshape(block_shape)
        for values in (query, keyed, valued, unit_key, decay_logarithm, rate)
    )
    cumul = jnp.cumsum(decay_b, axis=1)
    before = cumul - decay_b
    a_prime = -unit_b * jnp.exp(before)
    b_scaled = unit_b * rate_b * jnp.exp(-cumul)
    k_scaled = keyed_b * jnp.exp(-cumul)
    r_prime = query_b * jnp.exp(cumul)
    removal = jnp.where(strict, contract("cthn,cshn->chts", a_prime, b_scaled), 0.0)
    writes = jnp.where(strict, contract("cthn,cshn->chts", a_prime, k_scaled), 0.0)
    reads = jnp.where(inclusive, contract("cthn,cshn->chts", r_prime, b_scaled), 0.0)
    key_reads = jnp.where(inclusive, contract("cthn,cshn->chts", r_prime, k_scaled), 0.0)
    power = removal
    inverse = eye_block + removal
    reach = 2
    while reach < block_size:
        power = contract("chts,chsu->chtu", power, power)
        inverse = inverse + contract("chts,chsu->chtu", inverse, power)
        reach = reach * 2
    unit_solved = contract("chts,cshn->chtn", inverse, a_prime)
    free_solved = contract(
        "chts,chsv->chtv", inverse, contract("chts,cshv->chtv", writes, valued_b)
    )
    probe_raw = jnp.transpose(r_prime, (0, 2, 1, 3)) + contract(
        "chts,chsn->chtn", reads, unit_solved
    )
    free_read = contract("chts,chsv->chtv", reads, free_solved) + contract(
        "chts,cshv->chtv", key_reads, valued_b
    )
    closing = jnp.exp(cumul[:, -1])
    b_end = b_scaled * closing[:, None]
    k_end = k_scaled * closing[:, None]
    step_map = eye_heads[None] * closing[:, :, None, :] + contract(
        "chtj,cthk->chjk", unit_solved, b_end
    )
    constant = contract("chtv,cthk->chvk", free_solved, b_end) + contract(
        "cthv,cthk->chvk", valued_b, k_end
    )
    local_state = jnp.zeros((number_heads, head_dimension, head_dimension), jnp.float32)
    product = eye_heads
    entering_states = []
    entering_maps = []
    for index in range(count):
        entering_states.append(local_state)
        entering_maps.append(product)
        local_state = contract("hvk,hkj->hvj", local_state, step_map[index]) + constant[index]
        product = contract("hij,hjk->hik", product, step_map[index])
    stacked_states = jnp.stack(entering_states)
    stacked_maps = jnp.stack(entering_maps)
    recalled = contract("chvk,chtk->cthv", stacked_states, probe_raw) + jnp.transpose(
        free_read, (0, 2, 1, 3)
    )
    probe = contract("chjk,chtk->cthj", stacked_maps, probe_raw)
    head_shape = (sequence_length, number_heads, head_dimension)
    return (recalled.reshape(head_shape), probe.reshape(head_shape), local_state, product)


def mixer_local(
    normed,
    projected,
    decay_first_map,
    decay_second_map,
    channel_decay_offset,
    position_decay_offset,
    extra_log_decay,
    rate_first_map,
    rate_second_map,
    channel_rate_offset,
):
    query, keyed, valued = (rounded(values) for values in projected)
    sequence_length = normed.shape[0]
    number_heads = extra_log_decay.shape[1]
    head_dimension = query.shape[1] // number_heads
    decay_low = jnp.tanh(
        jnp.dot(normed, decay_first_map, preferred_element_type=jnp.float32)
    ).astype(jnp.bfloat16)
    decay_logits = (
        channel_decay_offset
        + jnp.dot(decay_low, decay_second_map, preferred_element_type=jnp.float32)
        + position_decay_offset[:, None]
    )
    decay_logarithm = -DECAY_FACTOR * jax.nn.sigmoid(decay_logits) + jnp.repeat(
        extra_log_decay, head_dimension, axis=1
    )
    rate_low = jnp.dot(normed, rate_first_map, preferred_element_type=jnp.float32).astype(
        jnp.bfloat16
    )
    rate = jax.nn.sigmoid(
        channel_rate_offset + jnp.dot(rate_low, rate_second_map, preferred_element_type=jnp.float32)
    )
    head_shape = (sequence_length, number_heads, head_dimension)
    query_per_head = query.reshape(head_shape)
    key_per_head = keyed.reshape(head_shape)
    value_per_head = valued.reshape(head_shape)
    unit_key = key_per_head * lax.rsqrt(
        jnp.sum(key_per_head * key_per_head, axis=2, keepdims=True) + KEY_EPS
    )
    recalled, probe, final_state, final_product = mixer_blocks(
        query_per_head,
        key_per_head,
        value_per_head,
        unit_key,
        decay_logarithm.reshape(head_shape),
        rate.reshape(head_shape),
    )
    return (
        (query_per_head, key_per_head, value_per_head),
        recalled,
        probe,
        final_state,
        final_product,
    )


def compose(earlier, later_map):
    return (
        contract("hij,hjk->hik", earlier[0], later_map[0]),
        contract("hij,hjk->hik", earlier[1], later_map[0]) + later_map[1],
    )


def shards(
    tokens,
    input_norm_gain,
    query_weight,
    key_weight,
    value_weight,
    decay_first_map,
    decay_second_map,
    channel_decay_offset,
    position_decay_offset,
    extra_log_decay,
    rate_first_map,
    rate_second_map,
    channel_rate_offset,
    own_term_weight,
    head_norm_gain,
    starting_state,
    outer_gate_weight,
    inner_gate_weight,
    signal_weight,
    convolution_taps,
    convolution_gain,
):
    whole = gathered_copies(tokens, "tp", 1)
    wide = whole.astype(jnp.float32)
    normed = (
        wide * lax.rsqrt(jnp.mean(wide * wide, axis=1, keepdims=True) + NORM_EPS) * input_norm_gain
    ).astype(jnp.bfloat16)
    sequence_length = normed.shape[0]
    accumulate = fold_rows(normed)
    empty = jnp.zeros((sequence_length, query_weight.shape[1]), jnp.float32)
    mixer_args = (
        decay_first_map,
        decay_second_map,
        channel_decay_offset,
        position_decay_offset,
        extra_log_decay,
        rate_first_map,
        rate_second_map,
        channel_rate_offset,
    )
    projected = accumulate(
        (empty, empty, empty),
        in_one_piece((query_weight, key_weight, value_weight), SP, 0, 1),
        jnp.int32(0),
    )
    mixer = mixer_local(normed, projected, *mixer_args)
    outer, inner, signal = accumulate(
        (empty, empty, empty),
        in_one_piece((outer_gate_weight, inner_gate_weight, signal_weight), SP, 0, 1),
        jnp.int32(0),
    )
    (query_per_head, key_per_head, value_per_head), recalled, probe, final_state, final_product = (
        mixer
    )
    number_heads, head_dimension = (query_per_head.shape[1], query_per_head.shape[2])
    eye_heads = jnp.broadcast_to(jnp.eye(head_dimension, dtype=jnp.float32), final_product.shape)
    prefix_map, prefix_state = entering_2(
        (final_product, final_state), SP, compose, (eye_heads, jnp.zeros_like(final_state))
    )
    entering = contract("hvk,hkj->hvj", starting_state, prefix_map) + prefix_state
    recalled = recalled + contract("hvk,thk->thv", entering, probe)
    center = recalled - jnp.mean(recalled, axis=2, keepdims=True)
    variance = jnp.mean(center * center, axis=2, keepdims=True)
    input_normed = (
        center
        * lax.rsqrt(variance + GROUP_EPS)
        * head_norm_gain.reshape(number_heads, head_dimension)
    )
    own_term = (
        jnp.sum(
            query_per_head * key_per_head * own_term_weight.reshape(number_heads, head_dimension),
            axis=2,
            keepdims=True,
        )
        * value_per_head
    )
    linear_attention_output = (
        (input_normed + own_term)
        .reshape(sequence_length, number_heads * head_dimension)
        .astype(jnp.bfloat16)
    )
    outer_f = rounded(outer)
    mixed_in = (rounded(inner) * rounded(signal)).astype(jnp.bfloat16)
    previous = from_behind(mixed_in[sequence_length - 2 :], SP, 1)
    padded = jnp.concatenate([previous, mixed_in], axis=0).astype(jnp.float32)
    taps = convolution_taps.astype(jnp.float32)
    gated = outer_f * (taps[0] * padded[:-2] + taps[1] * padded[1:-1] + taps[2] * padded[2:])
    squares = over_copies(jnp.sum(gated * gated, axis=1), "tp")
    channel_total = gated.shape[1] * lax.axis_size("tp")
    out_conv = (
        gated * lax.rsqrt(squares[:, None] / channel_total + NORM_EPS) * convolution_gain
    ).astype(jnp.bfloat16)
    return (linear_attention_output, out_conv)


def solution(mesh):
    torus = Mesh(mesh.devices.reshape(4, 4, 2, mesh.shape["tp"]), ("sp_0", "sp_1", "sp_2", "tp"))
    return jax.shard_map(
        shards,
        mesh=torus,
        in_specs=(
            P(SP, "tp"),
            P(),
            P(SP, "tp"),
            P(SP, "tp"),
            P(SP, "tp"),
            P(),
            P(None, "tp"),
            P("tp"),
            P(SP),
            P(SP, "tp"),
            P(),
            P(None, "tp"),
            P("tp"),
            P("tp"),
            P("tp"),
            P("tp", None, None),
            P(SP, "tp"),
            P(SP, "tp"),
            P(SP, "tp"),
            P(None, "tp"),
            P("tp"),
        ),
        out_specs=(P(SP, "tp"), P(SP, "tp")),
        check_vma=False,
    )
```

profile of v0, /device:TPU:1, one launch (start us, length us, event | category | flops | bytes accessed | tf_op | source)
XLA Modules:
  0.0 252.8 jit_solution(11160351308676476766)
XLA Ops:
  13.9 5.0 %all-to-all-start = ((bf16[4,256,1024]{1,2,0:T(8,128)(2,1)}), bf16[4,256,1024]{1,2,0:T(8,128)(2,1)S(1)}, u32[]{:S(2)}, u32[]{:S(2)}) async-start(bf16[4,256,1024]{1,2,0:T(8,128)(2,1)} %broadcast_in_dim.66), calls=%async_computation | async-start | bytes 4194304 | tf_op jit(solution)/shard_map/all_to_all | solution.py:19
  22.0 22.3 %all-to-all-done = bf16[4,256,1024]{1,2,0:T(8,128)(2,1)S(1)} async-done(((bf16[4,256,1024]{1,2,0:T(8,128)(2,1)}), bf16[4,256,1024]{1,2,0:T(8,128)(2,1)S(1)}, u32[]{:S(2)}, u32[]{:S(2)}) %all-to-all-start) | async-done | bytes 2097184 | tf_op jit(solution)/shard_map/all_to_all | solution.py:19
  46.7 3.0 %fusion.27 = f32[256,512]{1,0:T(8,128)S(1)} fusion(f32[256,512]{1,0:T(8,128)} %copy.123, bf16[128,512]{1,0:T(8,128)(2,1)S(1)} %copy-done.21, bf16[256,4096]{0,1:T(8,128)(2,1)} %fusion.14, bf16[4096,128]{1,0:T(8,128)(2,1)S(1)} %copy-done, f32[256]{0:T(256)S(1)} %copy-done.25, f32[512]{0:T(512)S(1)} %copy-done.23), kind=kOutput, calls=%fused_computation.46 | convolution fusion | flops 302940160 | bytes 4328448 | tf_op jit(solution)/shard_map/dot_general | solution.py:192
  50.0 2.8 %fusion.29 = f32[256,512]{1,0:T(8,128)S(1)} fusion(bf16[128,512]{1,0:T(8,128)(2,1)S(1)} %copy-done.22, bf16[256,4096]{0,1:T(8,128)(2,1)} %fusion.14, bf16[4096,128]{1,0:T(8,128)(2,1)} %param.31, f32[512]{0:T(512)S(1)} %copy-done.24), kind=kOutput, calls=%fused_computation.48 | convolution fusion | flops 302546944 | bytes 3803136 | tf_op jit(solution)/shard_map/dot_general | solution.py:202
  54.0 26.0 %fusion.184 = f32[4,64,8,64]{3,2,1,0:T(8,128)S(1)} fusion(f32[4,64,8,64]{3,2,1,0:T(8,128)S(1)} %reshape_reshape.14), kind=kOutput, calls=%fused_computation.247 | output fusion | flops 8257536 | bytes 1048576 | tf_op jit(solution)/shard_map/jit(cumsum)/reduce_window_sum | solution.py:116
  80.1 4.2 %fusion.38 = bf16[256,512]{1,0:T(8,128)(2,1)S(1)} fusion(bf16[256,4096]{0,1:T(8,128)(2,1)} %fusion.14, bf16[4096,1536]{1,0:T(8,128)(2,1)} %all-gather.9.cloned.1.call-done), kind=kOutput, calls=%fused_computation.53 | convolution fusion | flops 1073872896 | bytes 6553600 | tf_op jit(solution)/shard_map/dot_general | solution.py:91
  84.3 3.5 %fusion.35 = bf16[256,512]{1,0:T(8,128)(2,1)S(1)} fusion(bf16[256,4096]{0,1:T(8,128)(2,1)S(1)} %copy-done.8, bf16[4096,1536]{1,0:T(8,128)(2,1)} %all-gather.9.cloned.1.call-done), kind=kOutput, calls=%fused_computation.52 | convolution fusion | flops 1073872896 | bytes 6553600 | tf_op jit(solution)/shard_map/dot_general | solution.py:91
  87.9 4.5 %fusion.32 = bf16[256,512]{1,0:T(8,128)(2,1)} fusion(bf16[256,4096]{0,1:T(8,128)(2,1)S(1)} %copy-done.8, bf16[4096,1536]{1,0:T(8,128)(2,1)} %all-gather.9.cloned.1.call-done), kind=kOutput, calls=%fused_computation.51 | convolution fusion | flops 1073872896 | bytes 6553600 | tf_op jit(solution)/shard_map/dot_general | solution.py:91
  94.8 2.2 convert_multiply_fusion.1
  102.0 2.3 broadcast_multiply_fusion.1
  124.2 2.1 fusion.73
  130.4 2.2 convolution_select_fusion.3
  137.2 2.4 convolution_select_fusion
  149.9 3.0 %all-gather.3 = bf16[16,64,64]{2,1,0:T(8,128)(2,1)S(1)} all-gather(bf16[8,64,64]{2,1,0:T(8,128)(2,1)S(1)} %fusion.53), channel_id=5, replica_groups=mesh['sp_0'=4,'sp_1'=4,'sp_2'=2,'tp'=4] {'sp_2'}, dimensions={0}, use_global_device_ids=true | all-gather | bytes 196608 | tf_op jit(solution)/shard_map/all_gather | solution.py:52
  155.8 11.4 %all-gather.4 = bf16[32,64,64]{2,1,0:T(8,128)(2,1)S(1)} all-gather(bf16[8,64,64]{2,1,0:T(8,128)(2,1)S(1)} %get-tuple-element.26), channel_id=6, replica_groups=mesh['sp_0'=4,'sp_1'=4,'sp_2'=2,'tp'=4] {'sp_1'}, dimensions={0}, use_global_device_ids=true | all-gather | bytes 327680 | tf_op jit(solution)/shard_map/all_gather | solution.py:52
  167.7 9.9 %all-gather.1 = bf16[32,64,64]{2,1,0:T(8,128)(2,1)S(1)} all-gather(bf16[8,64,64]{2,1,0:T(8,128)(2,1)S(1)} %get-tuple-element.28), channel_id=3, replica_groups=mesh['sp_0'=4,'sp_1'=4,'sp_2'=2,'tp'=4] {'sp_1'}, dimensions={0}, use_global_device_ids=true | all-gather | bytes 327680 | tf_op jit(solution)/shard_map/all_gather | solution.py:52
  178.7 11.5 %all-gather.5 = bf16[32,64,64]{2,1,0:T(8,128)(2,1)S(1)} all-gather(bf16[8,64,64]{2,1,0:T(8,128)(2,1)S(1)} %get-tuple-element.30), channel_id=7, replica_groups=mesh['sp_0'=4,'sp_1'=4,'sp_2'=2,'tp'=4] {'sp_0'}, dimensions={0}, use_global_device_ids=true | all-gather | bytes 327680 | tf_op jit(solution)/shard_map/all_gather | solution.py:52
  191.2 11.4 %all-gather.2 = bf16[32,64,64]{2,1,0:T(8,128)(2,1)S(1)} all-gather(bf16[8,64,64]{2,1,0:T(8,128)(2,1)S(1)} %get-tuple-element.32), channel_id=4, replica_groups=mesh['sp_0'=4,'sp_1'=4,'sp_2'=2,'tp'=4] {'sp_0'}, dimensions={0}, use_global_device_ids=true | all-gather | bytes 327680 | tf_op jit(solution)/shard_map/all_gather | solution.py:52
  209.2 4.2 %fusion.47 = bf16[256,512]{1,0:T(8,128)(2,1)S(1)} fusion(bf16[256,4096]{0,1:T(8,128)(2,1)} %fusion.14, bf16[4096,1536]{1,0:T(8,128)(2,1)} %all-gather.11.cloned.1.call-done), kind=kOutput, calls=%fused_computation.56 | convolution fusion | flops 1073872896 | bytes 6553600 | tf_op jit(solution)/shard_map/dot_general | solution.py:91
  213.4 3.4 %fusion.44 = bf16[256,512]{1,0:T(8,128)(2,1)S(1)} fusion(bf16[256,4096]{0,1:T(8,128)(2,1)S(1)} %copy-done.9, bf16[4096,1536]{1,0:T(8,128)(2,1)} %all-gather.11.cloned.1.call-done), kind=kOutput, calls=%fused_computation.55 | convolution fusion | flops 1073872896 | bytes 6553600 | tf_op jit(solution)/shard_map/dot_general | solution.py:91
  217.0 13.6 %collective-permute-start = (bf16[2,512]{1,0:T(2,128)(2,1)S(1)}, bf16[2,512]{1,0:T(2,128)(2,1)S(1)}, u32[]{:S(2)}, u32[]{:S(2)}) collective-permute-start(bf16[2,512]{1,0:T(2,128)(2,1)S(1)} %slice.198), channel_id=1, source_target_pairs={{0,4},{4,8},{8,12},{12,16},{16,20},{20,24},{24,28},{28,32},{32,36}... | collective-permute-start | bytes 6152 | tf_op jit(solution)/shard_map/ppermute | solution.py:70
  230.6 4.3 %fusion.41 = bf16[256,512]{1,0:T(8,128)(2,1)} fusion(bf16[256,4096]{0,1:T(8,128)(2,1)S(1)} %copy-done.9, bf16[4096,1536]{1,0:T(8,128)(2,1)} %all-gather.11.cloned.1.call-done), kind=kOutput, calls=%fused_computation.54 | convolution fusion | flops 1073872896 | bytes 6553600 | tf_op jit(solution)/shard_map/dot_general | solution.py:91
  237.3 3.2 %all-to-all-start.1 = ((f32[4,1,256]{2,1,0:T(1,128)}), f32[4,1,256]{2,1,0:T(1,128)S(1)}, u32[]{:S(2)}, u32[]{:S(2)}) async-start(f32[4,1,256]{2,1,0:T(1,128)} %broadcast_in_dim.72), calls=%async_computation.1 | async-start | bytes 8192 | tf_op jit(solution)/shard_map/all_to_all | solution.py:19
  241.6 3.0 %all-to-all-done.1 = f32[4,1,256]{2,1,0:T(1,128)S(1)} async-done(((f32[4,1,256]{2,1,0:T(1,128)}), f32[4,1,256]{2,1,0:T(1,128)S(1)}, u32[]{:S(2)}, u32[]{:S(2)}) %all-to-all-start.1) | async-done | bytes 4128 | tf_op jit(solution)/shard_map/all_to_all | solution.py:19
  (164 shorter events, 75.8 us)
Async XLA Ops:
  7.2 39.5 %copy-start = (bf16[4096,128]{1,0:T(8,128)(2,1)S(1)}, bf16[4096,128]{1,0:T(8,128)(2,1)}, u32[]{:S(2)}) copy-start(bf16[4096,128]{1,0:T(8,128)(2,1)} %param.26) | copy-start | bytes 3145732
  7.2 72.9 %all-gather.9.cloned.1.call-start = ((), (), s32[]{:S(2)}) async-start(), calls=%async_computation.2 | async-start | bytes 12976128 | tf_op jit(solution)/shard_map/all_gather | solution.py:36
  9.2 200.0 %all-gather.11.cloned.1.call-start = ((), (), s32[]{:S(2)}) async-start(), calls=%async_computation.3 | async-start | bytes 12976128 | tf_op jit(solution)/shard_map/all_gather | solution.py:36
  11.0 7.8 %copy-start.17 = (f32[256,8]{0,1:T(8,128)S(1)}, f32[256,8]{0,1:T(8,128)}, u32[]{:S(2)}) copy-start(f32[256,8]{0,1:T(8,128)} %param.30) | copy-start | bytes 24580
  12.3 9.4 %copy-start.19 = (f32[512]{0:T(512)S(1)}, f32[512]{0:T(512)}, u32[]{:S(2)}) copy-start(f32[512]{0:T(512)} %param.34) | copy-start | bytes 6148
  12.3 9.5 %copy-start.20 = (f32[512]{0:T(512)S(1)}, f32[512]{0:T(512)}, u32[]{:S(2)}) copy-start(f32[512]{0:T(512)} %param.35) | copy-start | bytes 6148
  12.3 9.6 %copy-start.16 = (bf16[3,512]{1,0:T(4,128)(2,1)S(1)}, bf16[3,512]{1,0:T(4,128)(2,1)}, u32[]{:S(2)}) copy-start(bf16[3,512]{1,0:T(4,128)(2,1)} %param.40) | copy-start | bytes 9220
  13.9 31.0 %copy-start.15 = (f32[4096]{0:T(1024)S(1)}, f32[4096]{0:T(1024)}, u32[]{:S(2)}) copy-start(f32[4096]{0:T(1024)} %param.22) | copy-start | bytes 49156
  13.9 30.4 %all-to-all-start = ((bf16[4,256,1024]{1,2,0:T(8,128)(2,1)}), bf16[4,256,1024]{1,2,0:T(8,128)(2,1)S(1)}, u32[]{:S(2)}, u32[]{:S(2)}) async-start(bf16[4,256,1024]{1,2,0:T(8,128)(2,1)} %broadcast_in_dim.66), calls=%async_computation | async-start | bytes 4194304 | tf_op jit(solution)/shard_map/all_to_all | solution.py:19
  18.8 27.8 %copy-start.21 = (bf16[128,512]{1,0:T(8,128)(2,1)S(1)}, bf16[128,512]{1,0:T(8,128)(2,1)}, u32[]{:S(2)}) copy-start(bf16[128,512]{1,0:T(8,128)(2,1)} %param.27) | copy-start | bytes 393220
  18.8 27.8 %copy-start.23 = (f32[512]{0:T(512)S(1)}, f32[512]{0:T(512)}, u32[]{:S(2)}) copy-start(f32[512]{0:T(512)} %param.28) | copy-start | bytes 6148
  18.8 27.8 %copy-start.25 = (f32[256]{0:T(256)S(1)}, f32[256]{0:T(256)}, u32[]{:S(2)}) copy-start(f32[256]{0:T(256)} %param.29) | copy-start | bytes 3076
  80.1 4.2 %copy-start.8 = (bf16[256,4096]{0,1:T(8,128)(2,1)S(1)}, bf16[256,4096]{0,1:T(8,128)(2,1)}, u32[]{:S(2)}) copy-start(bf16[256,4096]{0,1:T(8,128)(2,1)} %fusion.14) | copy-start | bytes 6291460
  84.3 16.6 %copy-start.11 = (bf16[256,512]{1,0:T(8,128)(2,1)}, bf16[256,512]{1,0:T(8,128)(2,1)S(1)}, u32[]{:S(2)}) copy-start(bf16[256,512]{1,0:T(8,128)(2,1)S(1)} %fusion.38) | copy-start | bytes 786436
  87.9 4.5 %copy-start.13 = (bf16[256,512]{1,0:T(8,128)(2,1)}, bf16[256,512]{1,0:T(8,128)(2,1)S(1)}, u32[]{:S(2)}) copy-start(bf16[256,512]{1,0:T(8,128)(2,1)S(1)} %fusion.35) | copy-start | bytes 786436
  102.0 4.3 %copy-start.4 = (bf16[4,64,8,64]{3,2,1,0:T(8,128)(2,1)S(1)}, bf16[4,64,8,64]{3,2,1,0:T(8,128)(2,1)}, u32[]{:S(2)}) copy-start(bf16[4,64,8,64]{3,2,1,0:T(8,128)(2,1)} %reshape_reshape.16) | copy-start | bytes 786436
  139.7 4.8 %copy-start.3 = (f32[4,8,64,64]{3,2,1,0:T(8,128)S(1)}, f32[4,8,64,64]{3,2,1,0:T(8,128)}, u32[]{:S(2)}) copy-start(f32[4,8,64,64]{3,2,1,0:T(8,128)} %copy-done.2) | copy-start | bytes 1572868
  209.2 4.2 %copy-start.9 = (bf16[256,4096]{0,1:T(8,128)(2,1)S(1)}, bf16[256,4096]{0,1:T(8,128)(2,1)}, u32[]{:S(2)}) copy-start(bf16[256,4096]{0,1:T(8,128)(2,1)} %fusion.14) | copy-start | bytes 6291460
  217.0 18.4 %collective-permute-start = (bf16[2,512]{1,0:T(2,128)(2,1)S(1)}, bf16[2,512]{1,0:T(2,128)(2,1)S(1)}, u32[]{:S(2)}, u32[]{:S(2)}) collective-permute-start(bf16[2,512]{1,0:T(2,128)(2,1)S(1)} %slice.198), channel_id=1, source_target_pairs={{0,4},{4,8},{8,12},{12,16},{16,20},{20,24},{24,28},{28,32},{32,36}... | collective-permute-start | bytes 6152 | tf_op jit(solution)/shard_map/ppermute | solution.py:70
  230.6 4.3 %copy-start.12 = (bf16[256,512]{1,0:T(8,128)(2,1)S(1)}, bf16[256,512]{1,0:T(8,128)(2,1)}, u32[]{:S(2)}) copy-start(bf16[256,512]{1,0:T(8,128)(2,1)} %copy-done.11) | copy-start | bytes 786436
  230.6 4.5 %copy-start.10 = (f32[256,512]{1,0:T(8,128)S(1)}, f32[256,512]{1,0:T(8,128)}, u32[]{:S(2)}) copy-start(f32[256,512]{1,0:T(8,128)} %get-tuple-element.22) | copy-start | bytes 1572868
  230.6 14.8 %copy-start.1 = (bf16[4096,128]{1,0:T(8,128)(2,1)S(1)}, bf16[4096,128]{1,0:T(8,128)(2,1)}, u32[]{:S(2)}) copy-start(bf16[4096,128]{1,0:T(8,128)(2,1)} %param.26) | copy-start | bytes 3145732
  234.9 9.7 %copy-start.18 = (f32[512]{0:T(512)S(1)}, f32[512]{0:T(512)}, u32[]{:S(2)}) copy-start(f32[512]{0:T(512)} %param.41) | copy-start | bytes 6148
  237.3 7.4 %all-to-all-start.1 = ((f32[4,1,256]{2,1,0:T(1,128)}), f32[4,1,256]{2,1,0:T(1,128)S(1)}, u32[]{:S(2)}, u32[]{:S(2)}) async-start(f32[4,1,256]{2,1,0:T(1,128)} %broadcast_in_dim.72), calls=%async_computation.1 | async-start | bytes 8192 | tf_op jit(solution)/shard_map/all_to_all | solution.py:19
  (7 other events, 20.0 us)
Sparse Core Ops, SparseCore 0:
  10.2 66.5 all-gather.8
  79.1 62.3 all-gather.10
where the time goes:
time: 257 us; the launch traced here: 253 us
  matrix products  80.9 us (31%)
  blocking collectives  49.1 us (19%)
  other arithmetic  40.2 us (16%)
  waiting for transfers between devices  25.4 us (10%)
  starting transfers between devices  21.9 us (9%)
  local copies, waits for them, and re-layouts  19.8 us (8%)
  between operations  15.5 us (6%)
    dot_general x61, matrix products, contract(): return jnp.einsum(spec, left, right, precision=lax.Precision.HIGHEST)  50.9 us
    all_gather x6, blocking collectives, entering_2(): lax.all_gather(part.astype(kind), axis)  49.1 us
    another operation x1, other arithmetic, mixer_blocks(): cumul = jnp.cumsum(decay_b, axis=1)  26 us
    all_to_all x2, waiting for transfers between devices, copy_for_each(): return lax.all_to_all(copies, axis, split_axis=0, concat_axis=0, tiled=True)  25.4 us
    dot_general x6, matrix products, accumulate(): jnp.dot(normed, weight_piece, preferred_element_type=jnp.float32)  24.2 us
    ppermute x1, starting transfers between devices, from_behind(): return lax.ppermute(block, axis, route)  13.6 us
    all_to_all x2, starting transfers between devices, copy_for_each(): return lax.all_to_all(copies, axis, split_axis=0, concat_axis=0, tiled=True)  8.21 us
  transfers between devices with their start and end apart: 5, of which 2 were waited for; matrix products, arithmetic and copies ran while one was open for 51% of the time, Pallas kernels for 0%

commit v1 on v0

v1 whole, which is shorter than its diff:
```python
import jax
import jax.numpy as jnp
from jax import lax
from jax.experimental import pallas as pl
from jax.experimental.pallas import tpu as pltpu
from jax.sharding import Mesh
from jax.sharding import PartitionSpec as P

SP = ("sp_0", "sp_1", "sp_2")
MESH_IDS = pl.DeviceIdType.MESH
F32 = jnp.float32
BF16 = jnp.bfloat16

DECAY_FACTOR = 0.606531
NORM_EPS = 1e-06
GROUP_EPS = 0.00064
KEY_EPS = 1e-06

TOK = 256
HALO = 16
FEATS = 4096
BLK = 64
PAIRS = 4
OFFSETS = (0, -1, 1, 2)


def dot_nn(a, b):
    return lax.dot_general(a, b, (((1,), (0,)), ((), ())), preferred_element_type=F32)


def dot_nt(a, b):
    return lax.dot_general(a, b, (((1,), (1,)), ((), ())), preferred_element_type=F32)


def parts(a):
    high = a.astype(BF16)
    return high, (a - high.astype(F32)).astype(BF16)


def fine(dot, a, b):
    ah, al = parts(a)
    bh, bl = parts(b)
    return dot(ah, bh) + (dot(al, bh) + dot(ah, bl))


def exact_left(a, b):
    high, rest = parts(b)
    mid = (b - high.astype(F32) - rest.astype(F32)).astype(BF16)
    return dot_nn(a, high) + (dot_nn(a, rest) + dot_nn(a, mid))


def iota(shape, dim):
    return lax.broadcasted_iota(jnp.int32, shape, dim)


def same_head():
    return (iota((128, 128), 0) // 64) == (iota((128, 128), 1) // 64)


def diagonal_blocks(compact):
    return jnp.where(same_head(), jnp.concatenate([compact, compact], axis=0), 0.0)


def head_sums(values):
    ones = same_head().astype(F32).astype(BF16)
    high, rest = parts(values)
    return dot_nn(high, ones) + dot_nn(rest, ones)


def pair_local(q, k, v, decay, rate, cum):
    head = iota((TOK, 128), 1) // 64
    chunk_row = iota((TOK, 128), 0) // BLK
    row, col = iota((TOK, TOK), 0), iota((TOK, TOK), 1)
    within = (row // BLK) == (col // BLK)
    strict = within & (row > col)
    inclusive = within & (row >= col)
    unit = k * lax.rsqrt(head_sums(k * k) + KEY_EPS)
    grow = jnp.exp(-cum)
    a = -unit * jnp.exp(cum - decay)
    b = unit * rate
    r = q * jnp.exp(cum)
    a16, r16, v16 = a.astype(BF16), r.astype(BF16), v.astype(BF16)
    right = jnp.concatenate([(b * grow).astype(BF16), (k * grow).astype(BF16)], axis=0)
    zero = jnp.zeros((TOK, 128), BF16)
    probe = r
    free = jnp.zeros((TOK, 128), F32)
    solved = jnp.zeros((TOK, 256), F32)
    for h in range(2):
        mine = head == h
        a_h, r_h, v_h = (jnp.where(mine, t, zero) for t in (a16, r16, v16))
        top = dot_nt(a_h, right)
        power = jnp.where(strict, top[:, :TOK], 0.0).astype(BF16)
        writes = jnp.where(strict, top[:, TOK:], 0.0).astype(BF16)
        bottom = dot_nt(r_h, right)
        reads = jnp.where(inclusive, bottom[:, :TOK], 0.0).astype(BF16)
        key_reads = jnp.where(inclusive, bottom[:, TOK:], 0.0).astype(BF16)
        y = jnp.concatenate([jnp.where(mine, a, 0.0), dot_nn(writes, v_h)], axis=1)
        for level in range(6):
            y = y + dot_nn(power, y.astype(BF16))
            if level < 5:
                power = dot_nn(power, power).astype(BF16)
        read = dot_nn(reads, y.astype(BF16))
        probe = probe + read[:, :128]
        free = free + read[:, 128:] + dot_nn(key_reads, v_h)
        solved = solved + y
    lasts = [cum[BLK * (c + 1) - 1 : BLK * (c + 1), :] for c in range(TOK // BLK)]
    last = jnp.concatenate([jnp.broadcast_to(t, (BLK, 128)) for t in lasts], axis=0)
    fade = jnp.exp(last - cum)
    b_end, k_end = b * fade, k * fade
    in_chunk = [chunk_row == c for c in range(TOK // BLK)]
    b_wide = jnp.concatenate([jnp.where(m, b_end, 0.0) for m in in_chunk], axis=1)
    k_wide = jnp.concatenate([jnp.where(m, k_end, 0.0) for m in in_chunk], axis=1)
    maps = fine(dot_nn, solved.T, b_wide)
    gains = maps[128:] + fine(dot_nn, v.T, k_wide)
    eye = iota((128, 128), 0) == iota((128, 128), 1)
    state = chain = None
    recalled, probes = [], []
    for c in range(TOK // BLK):
        rows = slice(BLK * c, BLK * (c + 1))
        lanes = slice(128 * c, 128 * (c + 1))
        if c == 0:
            recalled.append(free[rows])
            probes.append(probe[rows])
        else:
            both = fine(dot_nt, probe[rows], jnp.concatenate([state, chain], axis=0))
            recalled.append(free[rows] + both[:, :128])
            probes.append(both[:, 128:])
        step = jnp.where(same_head(), maps[:128, lanes], 0.0)
        step = step + jnp.where(eye, jnp.broadcast_to(jnp.exp(lasts[c]), (128, 128)), 0.0)
        gain = jnp.where(same_head(), gains[:, lanes], 0.0)
        if c == 0:
            state, chain = gain, step
        else:
            both = fine(dot_nn, jnp.concatenate([state, chain], axis=0), step)
            state, chain = both[:128] + gain, both[128:]
    return (
        jnp.concatenate(recalled, axis=0),
        jnp.concatenate(probes, axis=0),
        state[:64] + state[64:],
        chain[:64] + chain[64:],
    )


def compose(earlier, later):
    both = fine(dot_nn, jnp.concatenate(earlier, axis=0), diagonal_blocks(later[0]))
    return both[:64], both[64:] + later[1]


def advance(state, later):
    return fine(dot_nn, state, diagonal_blocks(later[0])) + later[1]


def kernel(
    tokens,
    gain,
    wq,
    wk,
    wv,
    decay_first,
    decay_second,
    channel_decay,
    position_decay,
    extra_decay,
    rate_first,
    rate_second,
    channel_rate,
    own_weight,
    norm_gain,
    start_state,
    wo,
    wi,
    wsig,
    taps,
    conv_gain,
    lin_out,
    conv_out,
    gat_q,
    gat_c,
    raw,
    xn,
    low_d,
    low_r,
    acc,
    q_s,
    k_s,
    v_s,
    decay_s,
    rate_s,
    cum_s,
    rec_s,
    probe_s,
    st1,
    st2,
    st3,
    ent,
    sq_s,
    load_sem,
    tok_send,
    tok_recv,
    ici_send,
    ici_recv,
    d2d_send,
    d2d_recv,
    misc_send,
    misc_recv,
):
    z, y, c = (lax.axis_index(n) for n in SP)
    x = lax.axis_index("tp")

    def up(pos, offset):
        return lax.rem(pos + (offset + 4), 4)

    def at_x(o):
        return {"tp": up(x, o)}

    def at_y(o):
        return {"sp_1": up(y, o)}

    def at_z(o):
        return {"sp_0": up(z, o)}

    sibling = {"sp_2": 1 - c}
    rank = z * 8 + y * 2 + c
    after, before = lax.rem(rank + 1, 32), lax.rem(rank + 31, 32)

    def at_rank(r):
        return {"sp_0": r // 8, "sp_1": lax.rem(r // 2, 4), "sp_2": lax.rem(r, 2)}

    def push(src, dst, send, recv, device):
        copy = pltpu.make_async_remote_copy(
            src_ref=src,
            dst_ref=dst,
            send_sem=send,
            recv_sem=recv,
            device_id=device,
            device_id_type=MESH_IDS,
        )
        copy.start()
        return copy

    def arrived(region, recv):
        pltpu.make_async_copy(region, region, recv).wait()

    loads = [pltpu.make_async_copy(tokens, raw.at[x], load_sem.at[0])]
    for i, w in enumerate((wq, wk, wv)):
        loads.append(
            pltpu.make_async_copy(w, gat_q.at[rank, :, pl.ds(512 * i, 512)], load_sem.at[1 + i])
        )
    for i, w in enumerate((wo, wi, wsig)):
        loads.append(
            pltpu.make_async_copy(w, gat_c.at[rank, :, pl.ds(512 * i, 512)], load_sem.at[4 + i])
        )
    loads.append(pltpu.make_async_copy(decay_first, low_d, load_sem.at[7]))
    loads.append(pltpu.make_async_copy(rate_first, low_r, load_sem.at[8]))
    for load in loads:
        load.start()

    barrier = pltpu.get_barrier_semaphore()
    partners = [at_x(o) for o in OFFSETS[1:]] + [at_y(o) for o in OFFSETS[1:]]
    partners += [at_z(o) for o in OFFSETS[1:]] + [sibling, at_rank(after), at_rank(before)]
    for partner in partners:
        pl.semaphore_signal(barrier, inc=1, device_id=partner, device_id_type=MESH_IDS)
    pl.semaphore_wait(barrier, len(partners))

    loads[0].wait()
    tok_copies = [
        push(raw.at[x], raw.at[x], tok_send.at[0], tok_recv.at[0], at_x(1)),
        push(raw.at[x], raw.at[x], tok_send.at[1], tok_recv.at[1], at_x(-1)),
    ]

    def token_forward():
        left, right = up(x, -1), up(x, 1)
        arrived(raw.at[left], tok_recv.at[0])
        part = raw.at[left, pl.ds(0, 128)]
        tok_copies.append(push(part, part, tok_send.at[2], tok_recv.at[2], at_x(1)))
        arrived(raw.at[right], tok_recv.at[1])
        part = raw.at[right, pl.ds(128, 128)]
        tok_copies.append(push(part, part, tok_send.at[3], tok_recv.at[3], at_x(-1)))

    def token_rest():
        far = up(x, 2)
        arrived(raw.at[far, pl.ds(0, 128)], tok_recv.at[2])
        arrived(raw.at[far, pl.ds(128, 128)], tok_recv.at[3])

    class Gather:
        def __init__(self, which, buf):
            self.g, self.buf = which, buf

        def block(self, half, a, b, core):
            dy, dz = (a, b) if half == 0 else (b, a)
            return up(z, dz) * 8 + up(y, dy) * 2 + core

        def region(self, half, a, b, first, count, core=None):
            block = self.block(half, a, b, c if core is None else core)
            return self.buf.at[block, pl.ds(half * 64 + first, count)]

        def recv(self, half, index):
            return ici_recv.at[self.g * 40 + half * 20 + index]

        def send(self, half, along_a, direction, region, index):
            device = (at_y if (half == 0) == along_a else at_z)(direction)
            push(region, region, ici_send.at[self.g], self.recv(half, index), device)

        def share(self, half, ai, bi):
            region = self.region(half, OFFSETS[ai], OFFSETS[bi], 0, 64)
            sem = d2d_recv.at[self.g * 32 + half * 16 + ai * 4 + bi]
            push(region, region, d2d_send.at[self.g], sem, sibling)

        def spread(self, half, ai):
            region = self.region(half, OFFSETS[ai], 0, 0, 64)
            self.send(half, False, 1, region, 4 + 4 * ai)
            self.send(half, False, -1, region, 5 + 4 * ai)

        def start(self):
            for half in range(2):
                region = self.region(half, 0, 0, 0, 64)
                self.send(half, True, 1, region, 0)
                self.send(half, True, -1, region, 1)
            for half in range(2):
                self.spread(half, 0)
                self.share(half, 0, 0)

        def first_near(self, half, j):
            offset = (-1, 1)[j]
            arrived(self.region(half, offset, 0, 0, 64), self.recv(half, j))
            self.send(half, True, -offset, self.region(half, offset, 0, 32 * j, 32), 2 + j)
            self.spread(half, 1 + j)
            self.share(half, 1 + j, 0)

        def first_far(self, half):
            for j in range(2):
                arrived(self.region(half, 2, 0, 32 * j, 32), self.recv(half, 2 + j))
            self.spread(half, 3)
            self.share(half, 3, 0)

        def second_near(self, half, ai, j):
            offset = (-1, 1)[j]
            a = OFFSETS[ai]
            arrived(self.region(half, a, offset, 0, 64), self.recv(half, 4 + 4 * ai + j))
            part = self.region(half, a, offset, 32 * j, 32)
            self.send(half, False, -offset, part, 6 + 4 * ai + j)
            self.share(half, ai, 1 + j)

        def second_far(self, half, ai):
            for j in range(2):
                region = self.region(half, OFFSETS[ai], 2, 32 * j, 32)
                arrived(region, self.recv(half, 6 + 4 * ai + j))
            self.share(half, ai, 3)

        def shared(self, dy, dz):
            for half in range(2):
                a, b = (dy, dz) if half == 0 else (dz, dy)
                index = half * 16 + OFFSETS.index(a) * 4 + OFFSETS.index(b)
                region = self.region(half, a, b, 0, 64, 1 - c)
                arrived(region, d2d_recv.at[self.g * 32 + index])

        def steps(self):
            groups = []
            groups.append([lambda h=h, j=j: self.first_near(h, j) for j in (0, 1) for h in (0, 1)])
            groups.append(
                [lambda h=h, j=j: self.second_near(h, 0, j) for j in (0, 1) for h in (0, 1)]
            )
            groups.append([lambda h=h: self.first_far(h) for h in (0, 1)])
            groups.append(
                [
                    lambda h=h, j=j, a=a: self.second_near(h, a, j)
                    for a in (1, 2)
                    for j in (0, 1)
                    for h in (0, 1)
                ]
            )
            groups.append([lambda h=h: self.second_far(h, 0) for h in (0, 1)])
            groups.append(
                [lambda h=h, j=j: self.second_near(h, 3, j) for j in (0, 1) for h in (0, 1)]
            )
            groups.append([lambda h=h, a=a: self.second_far(h, a) for a in (1, 2, 3) for h in (0, 1)])
            return groups

        def finish(self):
            arrived(self.buf.at[pl.ds(0, 15)], ici_send.at[self.g])
            arrived(self.buf.at[pl.ds(0, 16)], d2d_send.at[self.g])

    def run(group):
        for step in group:
            step()

    near = [(dy, dz) for dy in (0, -1, 1) for dz in (0, -1, 1)]
    far = [(dy, dz) for dy in OFFSETS for dz in OFFSETS if 2 in (dy, dz)]

    def multiply(gather, chips, first_row, fresh):
        rows = TOK + HALO - first_row
        for n, (dy, dz) in enumerate(chips):
            gather.shared(dy, dz)
            chip = up(z, dz) * 4 + up(y, dy)
            left = xn[chip, pl.ds(first_row, rows)]
            right = gather.buf[pl.ds(chip * 2, 2)].reshape(256, 1536)
            part = dot_nn(left, right)
            if fresh and n == 0:
                acc[pl.ds(first_row, rows)] = part
            else:
                acc[pl.ds(first_row, rows)] += part

    gather_q, gather_c = Gather(0, gat_q), Gather(1, gat_c)
    for load in loads[1:4]:
        load.wait()
    gather_q.start()
    steps_q = gather_q.steps()
    run(steps_q[0])
    run(steps_q[1])
    token_forward()
    run(steps_q[2])
    run(steps_q[3][:4])
    token_rest()

    total = jnp.zeros((TOK, 1), F32)
    for i in range(4):
        wide = raw[i].astype(F32)
        total = total + jnp.sum(wide * wide, axis=1, keepdims=True)
    inverse = lax.rsqrt(total / FEATS + NORM_EPS)
    for i in range(4):
        for j in range(4):
            lanes = slice(256 * j, 256 * (j + 1))
            wide = raw[i, :, lanes].astype(F32) * inverse * gain[:, 1024 * i + 256 * j :][:, :256]
            xn[4 * i + j, pl.ds(HALO, TOK)] = wide.astype(BF16)
    run(steps_q[3][4:])
    run(steps_q[4])
    edge = pl.ds(TOK, HALO)
    halo_copy = push(
        xn.at[:, edge], xn.at[:, pl.ds(0, HALO)], misc_send.at[0], misc_recv.at[0], at_rank(after)
    )

    loads[7].wait()
    loads[8].wait()
    low = jnp.zeros((TOK, 256), F32)
    for i in range(16):
        rows = pl.ds(256 * i, 256)
        both = jnp.concatenate([low_d[rows], low_r[rows]], axis=1)
        low = low + dot_nn(xn[i, pl.ds(HALO, TOK)], both)
    decay_low = jnp.tanh(low[:, :128]).astype(BF16)
    rate_low = low[:, 128:].astype(BF16)
    by_position = jnp.broadcast_to(position_decay[...], (128, TOK)).T
    for p in range(PAIRS):
        lanes = slice(128 * p, 128 * (p + 1))
        logits = channel_decay[:, lanes] + dot_nn(decay_low, decay_second[:, lanes]) + by_position
        extra = jnp.where(
            iota((TOK, 128), 1) < 64,
            extra_decay[:, 2 * p : 2 * p + 1],
            extra_decay[:, 2 * p + 1 : 2 * p + 2],
        )
        decay_s[p] = -DECAY_FACTOR * jax.nn.sigmoid(logits) + extra
        rate_s[p] = jax.nn.sigmoid(
            channel_rate[:, lanes] + dot_nn(rate_low, rate_second[:, lanes])
        )
    row, col = iota((TOK, TOK), 0), iota((TOK, TOK), 1)
    summing = (((row // BLK) == (col // BLK)) & (row >= col)).astype(F32).astype(BF16)
    for p in range(PAIRS):
        cum_s[p] = exact_left(summing, decay_s[p])

    multiply(gather_q, near[:4], HALO, True)
    run(steps_q[5])
    for load in loads[4:7]:
        load.wait()
    gather_c.start()
    multiply(gather_q, near[4:], HALO, False)
    run(steps_q[6])
    multiply(gather_q, far, HALO, False)
    body = pl.ds(HALO, TOK)
    for p in range(PAIRS):
        for i, dst in enumerate((q_s, k_s, v_s)):
            rounded = acc[body, 512 * i + 128 * p : 512 * i + 128 * (p + 1)].astype(BF16)
            dst[p] = rounded.astype(F32)

    steps_c = gather_c.steps()
    during = {1: steps_c[0], 2: steps_c[1], 3: steps_c[2]}

    def one_pair(p, carry):
        for at, group in during.items():
            pl.when(p == at)(lambda group=group: run(group))
        recalled, probe, state, chain = pair_local(
            q_s[p], k_s[p], v_s[p], decay_s[p], rate_s[p], cum_s[p]
        )
        rec_s[p] = recalled
        probe_s[p] = probe
        st1[c, 2 * p] = chain.astype(BF16)
        st1[c, 2 * p + 1] = state.astype(BF16)
        return carry

    lax.fori_loop(0, PAIRS, one_pair, 0)

    copies = [push(st1.at[c], st1.at[c], misc_send.at[1], misc_recv.at[1], sibling)]
    run(steps_c[3])
    arrived(st1.at[1 - c], misc_recv.at[1])

    def held(ref, slot, p):
        return ref[slot, 2 * p].astype(F32), ref[slot, 2 * p + 1].astype(F32)

    for n in range(2):
        p = 2 * c + n
        chain, state = compose(held(st1, 0, p), held(st1, 1, p))
        st2[y, 2 * n] = chain.astype(BF16)
        st2[y, 2 * n + 1] = state.astype(BF16)
    for i, o in enumerate(OFFSETS[1:]):
        copies.append(push(st2.at[y], st2.at[y], misc_send.at[2 + i], misc_recv.at[2 + i], at_y(o)))
    run(steps_c[4])
    for i, o in enumerate(OFFSETS[1:]):
        arrived(st2.at[up(y, -o)], misc_recv.at[2 + i])
    ahead = []
    for n in range(2):
        total_map = held(st2, 0, n)
        eye = (iota((64, 128), 0) == lax.rem(iota((64, 128), 1), 64)).astype(F32)
        prefix = (eye, jnp.zeros((64, 128), F32))
        for k in range(1, 4):
            prefix = tuple(jnp.where(y >= k, new, old) for new, old in zip(total_map, prefix))
            total_map = compose(total_map, held(st2, k, n))
        ahead.append(prefix)
        st3[z, 2 * n] = total_map[0].astype(BF16)
        st3[z, 2 * n + 1] = total_map[1].astype(BF16)
    for i, o in enumerate(OFFSETS[1:]):
        copies.append(push(st3.at[z], st3.at[z], misc_send.at[5 + i], misc_recv.at[5 + i], at_z(o)))
    run(steps_c[5])
    for i, o in enumerate(OFFSETS[1:]):
        arrived(st3.at[up(z, -o)], misc_recv.at[5 + i])
    for n in range(2):
        p = 2 * c + n
        state = jnp.concatenate([start_state[2 * p], start_state[2 * p + 1]], axis=1)
        for k in range(3):
            state = jnp.where(z > k, advance(state, held(st3, k, n)), state)
        ent[p] = advance(state, ahead[n])
    copies.append(
        push(
            ent.at[pl.ds(2 * c, 2)],
            ent.at[pl.ds(2 * c, 2)],
            misc_send.at[8],
            misc_recv.at[8],
            sibling,
        )
    )
    arrived(xn.at[:, pl.ds(0, HALO)], misc_recv.at[0])
    halo = xn[:, pl.ds(0, HALO)]
    xn[:, pl.ds(0, HALO)] = jnp.where(rank == 0, jnp.zeros_like(halo), halo)
    multiply(gather_c, near, 0, True)
    arrived(ent.at[pl.ds(2 * (1 - c), 2)], misc_recv.at[8])
    for p in range(PAIRS):
        lanes = slice(128 * p, 128 * (p + 1))
        state = ent[p]
        state = jnp.where(c == 1, advance(state, held(st1, 0, p)), state)
        recalled = rec_s[p] + fine(dot_nt, probe_s[p], diagonal_blocks(state))
        center = recalled - head_sums(recalled) * (1.0 / 64)
        variance = head_sums(center * center) * (1.0 / 64)
        normed = center * lax.rsqrt(variance + GROUP_EPS) * norm_gain[:, lanes]
        own = head_sums(q_s[p] * k_s[p] * own_weight[:, lanes]) * v_s[p]
        lin_out[:, lanes] = (normed + own).astype(BF16)

    run(steps_c[6])
    multiply(gather_c, far, 0, False)
    squares = jnp.zeros((TOK, 128), F32)
    for p in range(PAIRS):
        lanes = slice(128 * p, 128 * (p + 1))
        outer, inner, signal = (
            acc[:, 512 * i + 128 * p : 512 * i + 128 * (p + 1)].astype(BF16).astype(F32)
            for i in range(3)
        )
        mixed = (inner * signal).astype(BF16).astype(F32)
        tap = taps[:, lanes].astype(F32)
        gated = outer[HALO:] * (
            tap[0:1] * pltpu.roll(mixed, 2, 0)[HALO:]
            + tap[1:2] * pltpu.roll(mixed, 1, 0)[HALO:]
            + tap[2:3] * mixed[HALO:]
        )
        q_s[p] = gated
        squares = squares + gated * gated
    column = jnp.broadcast_to(jnp.sum(squares, axis=1, keepdims=True), (TOK, 128))
    sq_s[x] = column.T[:8]
    for i, o in enumerate(OFFSETS[1:]):
        copies.append(push(sq_s.at[x], sq_s.at[x], misc_send.at[9 + i], misc_recv.at[9 + i], at_x(o)))
    gather_q.finish()
    gather_c.finish()
    for copy in tok_copies:
        copy.wait_send()
    halo_copy.wait_send()
    for i, o in enumerate(OFFSETS[1:]):
        arrived(sq_s.at[up(x, -o)], misc_recv.at[9 + i])
    summed = sq_s[0] + sq_s[1] + sq_s[2] + sq_s[3]
    column = jnp.concatenate([summed] * 16, axis=0).T
    scale = lax.rsqrt(column / 2048 + NORM_EPS)
    for p in range(PAIRS):
        lanes = slice(128 * p, 128 * (p + 1))
        conv_out[:, lanes] = (q_s[p] * scale * conv_gain[:, lanes]).astype(BF16)
    for copy in copies:
        copy.wait_send()


def shards(
    tokens,
    input_norm_gain,
    query_weight,
    key_weight,
    value_weight,
    decay_first_map,
    decay_second_map,
    channel_decay_offset,
    position_decay_offset,
    extra_log_decay,
    rate_first_map,
    rate_second_map,
    channel_rate_offset,
    own_term_weight,
    head_norm_gain,
    starting_state,
    outer_gate_weight,
    inner_gate_weight,
    signal_weight,
    convolution_taps,
    convolution_gain,
):
    far = pl.BlockSpec(memory_space=pl.ANY)
    near = pl.BlockSpec(memory_space=pltpu.VMEM)

    def line(v):
        return v.reshape(1, -1)

    pair = pltpu.VMEM((PAIRS, TOK, 128), F32)
    dma = pltpu.SemaphoreType.DMA
    out = jax.ShapeDtypeStruct((TOK, 512), BF16)
    return pl.pallas_call(
        kernel,
        name="mixer",
        out_shape=(out, out),
        in_specs=[far, near, far, far, far, far, near, near, near, near, far]
        + [near] * 5
        + [far, far, far, near, near],
        out_specs=(near, near),
        scratch_shapes=[
            pltpu.VMEM((32, 128, 1536), BF16),
            pltpu.VMEM((32, 128, 1536), BF16),
            pltpu.VMEM((4, TOK, 1024), BF16),
            pltpu.VMEM((16, TOK + HALO, 256), BF16),
            pltpu.VMEM((FEATS, 128), BF16),
            pltpu.VMEM((FEATS, 128), BF16),
            pltpu.VMEM((TOK + HALO, 1536), F32),
        ]
        + [pair] * 8
        + [
            pltpu.VMEM((2, 8, 64, 128), BF16),
            pltpu.VMEM((4, 4, 64, 128), BF16),
            pltpu.VMEM((4, 4, 64, 128), BF16),
            pltpu.VMEM((PAIRS, 64, 128), F32),
            pltpu.VMEM((4, 8, TOK), F32),
            dma((9,)),
            dma((4,)),
            dma((4,)),
            dma((2,)),
            dma((80,)),
            dma((2,)),
            dma((64,)),
            dma((12,)),
            dma((12,)),
        ],
        compiler_params=pltpu.CompilerParams(
            collective_id=0, has_side_effects=True, vmem_limit_bytes=60 * 1024 * 1024
        ),
    )(
        tokens,
        line(input_norm_gain),
        query_weight,
        key_weight,
        value_weight,
        decay_first_map,
        decay_second_map,
        line(channel_decay_offset),
        line(position_decay_offset),
        extra_log_decay,
        rate_first_map,
        rate_second_map,
        line(channel_rate_offset),
        line(own_term_weight),
        line(head_norm_gain),
        starting_state,
        outer_gate_weight,
        inner_gate_weight,
        signal_weight,
        convolution_taps,
        line(convolution_gain),
    )


def solution(mesh):
    torus = Mesh(mesh.devices.reshape(4, 4, 2, mesh.shape["tp"]), (*SP, "tp"))
    return jax.shard_map(
        shards,
        mesh=torus,
        in_specs=(
            P(SP, "tp"),
            P(),
            P(SP, "tp"),
            P(SP, "tp"),
            P(SP, "tp"),
            P(),
            P(None, "tp"),
            P("tp"),
            P(SP),
            P(SP, "tp"),
            P(),
            P(None, "tp"),
            P("tp"),
            P("tp"),
            P("tp"),
            P("tp", None, None),
            P(SP, "tp"),
            P(SP, "tp"),
            P(SP, "tp"),
            P(None, "tp"),
            P("tp"),
        ),
        out_specs=(P(SP, "tp"), P(SP, "tp")),
        check_vma=False,
    )
```

time: 257 us -> 103 us (0.40); the launches traced: 253 us -> 103 us
  Pallas kernels: 0 us -> 98.2 us
  matrix products: 80.9 us -> 0 us
  blocking collectives: 49.1 us -> 0 us
  other arithmetic: 40.2 us -> 0 us
  waiting for transfers between devices: 25.4 us -> 0 us
  starting transfers between devices: 21.9 us -> 0 us
  local copies, waits for them, and re-layouts: 19.8 us -> 3.9 us
  between operations: 15.5 us -> 0.66 us
    pallas_call x0 -> x1, Pallas kernels: none -> 98.2 us  [shards(): pl.pallas_call(kernel, name='mixer', out_shape=(out, out), in_specs=[far,...]
    dot_general x69 -> x0, matrix products: 80.9 us -> none  [the longest x61 50.9 us: contract(): return jnp.einsum(spec, left, right, precision=lax.Precision.HIGHEST)]
    all_gather x6 -> x0, blocking collectives: 49.1 us -> none  [entering_2(): lax.all_gather(part.astype(kind), axis)]
    another operation x1 -> x0, other arithmetic: 26 us -> none  [mixer_blocks(): cumul = jnp.cumsum(decay_b, axis=1)]
    all_to_all x2 -> x0, waiting for transfers between devices: 25.4 us -> none  [copy_for_each(): return lax.all_to_all(copies, axis, split_axis=0, concat_axis=0, tiled=True)]
    ppermute x1 -> x0, starting transfers between devices: 13.6 us -> none  [from_behind(): return lax.ppermute(block, axis, route)]
    all_to_all x2 -> x0, starting transfers between devices: 8.21 us -> none  [copy_for_each(): return lax.all_to_all(copies, axis, split_axis=0, concat_axis=0, tiled=True)]
    reshape x5 -> x0, local copies, waits for them, and re-layouts: 5.47 us -> none  [the longest x1 2.04 us: mixer_local(): jnp.repeat(extra_log_decay, head_dimension, axis=1)]
  transfers between devices with their start and end apart: 5 -> 0, of which waited for: 2 -> 0; matrix products, arithmetic and copies ran while one was open for 51% -> 0% of each run, Pallas kernels for 0% -> 0%
where the time goes in v1:
time: 103 us
  Pallas kernels  98.2 us (95%)
  local copies, waits for them, and re-layouts  3.9 us (4%)
    pallas_call x1, Pallas kernels, shards(): pl.pallas_call(kernel, name='mixer', out_shape=(out, out), in_specs=[far,...  98.2 us
    unnamed x7, local copies, waits for them, and re-layouts  3.9 us

profile of v1, /device:TPU:1, one launch (start us, length us, event | category | flops | bytes accessed | tf_op | source)
XLA Modules:
  0.0 102.8 jit_solution(6310043419012511055)
XLA Ops:
  0.6 0.0 copy-start.1
  0.6 0.7 copy-done.1
  1.3 0.8 copy.23.extra_decay
  2.1 98.2 %mixer.1 = (bf16[256,512]{1,0:T(8,128)(2,1)}, bf16[256,512]{1,0:T(8,128)(2,1)}) custom-call(bf16[256,1024]{1,0:T(8,128)(2,1)} %tokens.1, f32[1,4096]{1,0:T(1,128)} %bitcast.7, bf16[128,512]{1,0:T(8,128)(2,1)} %wq.1, bf16[128,512]{1,0:T(8,128)(2,1)} %wk.1, bf16[128,512]{1,0:T(8,128)(2,1)} %wv.1, bf16[4096,128]{1,0:T(8,128)(2,1)} %decay_first.1, ...), custom_call_target="tpu_custom_call" | custom-call | tf_op jit(solution)/shard_map/mixer/pallas_call | solution.py:625
  100.3 0.0 copy-start
  100.3 1.7 %copy.26 = bf16[256,512]{1,0:T(8,128)(2,1)} copy(bf16[256,512]{1,0:T(8,128)(2,1)} %get-tuple-element.4) | data formatting | bytes 524288
  102.1 0.0 copy-done
  102.1 0.7 copy.27
Async XLA Ops:
  0.6 0.7 copy-start.1
  100.3 1.7 %copy-start = (bf16[256,512]{1,0:T(8,128)(2,1)S(1)}, bf16[256,512]{1,0:T(8,128)(2,1)}, u32[]{:S(2)}) copy-start(bf16[256,512]{1,0:T(8,128)(2,1)} %get-tuple-element.5) | copy-start | bytes 786436

commit v2 on v1

v2 whole, which is shorter than its diff:
```python
import jax
import jax.numpy as jnp
from jax import lax
from jax.experimental import pallas as pl
from jax.experimental.pallas import tpu as pltpu
from jax.sharding import Mesh
from jax.sharding import PartitionSpec as P

SP = ("sp_0", "sp_1", "sp_2")
MESH_IDS = pl.DeviceIdType.MESH
F32 = jnp.float32
BF16 = jnp.bfloat16

DECAY_FACTOR = 0.606531
NORM_EPS = 1e-06
GROUP_EPS = 0.00064
KEY_EPS = 1e-06

TOK = 256
HALO = 16
FEATS = 4096
BLK = 64
PAIRS = 4
OFFSETS = (0, -1, 1, 2)


def dot_nn(a, b):
    return lax.dot_general(a, b, (((1,), (0,)), ((), ())), preferred_element_type=F32)


def dot_nt(a, b):
    return lax.dot_general(a, b, (((1,), (1,)), ((), ())), preferred_element_type=F32)


def parts(a):
    high = a.astype(BF16)
    return high, (a - high.astype(F32)).astype(BF16)


def dot_tn(a, b):
    return lax.dot_general(a, b, (((0,), (0,)), ((), ())), preferred_element_type=F32)


def fine(dot, a, b):
    ah, al = parts(a)
    bh, bl = parts(b)
    a_dim = 0 if dot is dot_tn else 1
    b_dim = 1 if dot is dot_nt else 0
    return dot(
        jnp.concatenate([ah, al, ah], axis=a_dim), jnp.concatenate([bh, bh, bl], axis=b_dim)
    )


def exact_left(a, b):
    high, rest = parts(b)
    mid = (b - high.astype(F32) - rest.astype(F32)).astype(BF16)
    return dot_nn(a, high) + (dot_nn(a, rest) + dot_nn(a, mid))


def iota(shape, dim):
    return lax.broadcasted_iota(jnp.int32, shape, dim)


def same_head():
    return (iota((128, 128), 0) // 64) == (iota((128, 128), 1) // 64)


def diagonal_blocks(compact):
    return jnp.where(same_head(), jnp.concatenate([compact, compact], axis=0), 0.0)


def head_sums(values):
    ones = same_head().astype(F32).astype(BF16)
    high, rest = parts(values)
    return dot_nn(high, ones) + dot_nn(rest, ones)


def spread_heads(values):
    both = jnp.concatenate([values, values], axis=0)
    return jnp.where(same_head(), both, jnp.zeros_like(both))


def pair_local(q, k, v, decay, rate, cum):
    chunks = range(TOK // BLK)
    rows = [slice(BLK * n, BLK * (n + 1)) for n in chunks]
    later, earlier = iota((BLK, 128), 0), lax.rem(iota((BLK, 128), 1), BLK)
    strict, inclusive = later > earlier, later >= earlier
    unit = k * lax.rsqrt(head_sums(k * k) + KEY_EPS)
    grow = jnp.exp(-cum)
    a = -unit * jnp.exp(cum - decay)
    b = unit * rate
    r = q * jnp.exp(cum)
    a16, r16, v16 = a.astype(BF16), r.astype(BF16), v.astype(BF16)
    b16, k16 = (b * grow).astype(BF16), (k * grow).astype(BF16)
    grams = [
        dot_nt(
            jnp.concatenate([a16[t], r16[t]], axis=0),
            jnp.concatenate([spread_heads(b16[t]), spread_heads(k16[t])], axis=0),
        )
        for t in rows
    ]
    power = [jnp.where(strict, g[:BLK, :128], 0.0).astype(BF16) for g in grams]
    writes = [jnp.where(strict, g[:BLK, 128:], 0.0).astype(BF16) for g in grams]
    reads = [
        jnp.concatenate(
            [
                jnp.where(inclusive, g[BLK:, :128], 0.0).astype(BF16),
                jnp.where(inclusive, g[BLK:, 128:], 0.0).astype(BF16),
            ],
            axis=1,
        )
        for g in grams
    ]
    values = [spread_heads(v16[t]) for t in rows]
    keys_solved = [a[t] for t in rows]
    free_solved = [dot_nn(writes[n], values[n]) for n in chunks]
    for level in range(6):
        for n in chunks:
            right = [spread_heads(keys_solved[n].astype(BF16))]
            right.append(spread_heads(free_solved[n].astype(BF16)))
            if level < 5:
                right.append(spread_heads(power[n]))
            product = dot_nn(power[n], jnp.concatenate(right, axis=1))
            keys_solved[n] = keys_solved[n] + product[:, :128]
            free_solved[n] = free_solved[n] + product[:, 128:256]
            if level < 5:
                power[n] = product[:, 256:].astype(BF16)
    read = []
    for n in chunks:
        top = [spread_heads(keys_solved[n].astype(BF16)), spread_heads(free_solved[n].astype(BF16))]
        low = [jnp.zeros((128, 128), BF16), values[n]]
        right = jnp.concatenate([jnp.concatenate(t, axis=1) for t in (top, low)], axis=0)
        read.append(dot_nn(reads[n], right))
    eye = iota((128, 128), 0) == iota((128, 128), 1)
    steps, gains = [], []
    for n in chunks:
        last = cum[BLK * (n + 1) - 1 : BLK * (n + 1), :]
        fade = jnp.exp(last - cum[rows[n]])
        b_end, k_end = b[rows[n]] * fade, k[rows[n]] * fade
        solved = jnp.concatenate([keys_solved[n], free_solved[n]], axis=1)
        both = fine(dot_tn, solved, b_end)
        step = jnp.where(same_head(), both[:128], 0.0)
        steps.append(step + jnp.where(eye, jnp.broadcast_to(jnp.exp(last), (128, 128)), 0.0))
        gain = both[128:] + fine(dot_tn, v[rows[n]], k_end)
        gains.append(jnp.where(same_head(), gain, 0.0))
    state, chain = gains[0], steps[0]
    recalled, probes = [read[0][:, 128:]], [r[rows[0]] + read[0][:, :128]]
    for n in chunks[1:]:
        carried = jnp.concatenate([state, chain], axis=0)
        both = fine(dot_nt, r[rows[n]] + read[n][:, :128], carried)
        recalled.append(read[n][:, 128:] + both[:, :128])
        probes.append(both[:, 128:])
        both = fine(dot_nn, carried, steps[n])
        state, chain = both[:128] + gains[n], both[128:]
    return (
        jnp.concatenate(recalled, axis=0),
        jnp.concatenate(probes, axis=0),
        state[:64] + state[64:],
        chain[:64] + chain[64:],
    )


def compose(earlier, later):
    both = fine(dot_nn, jnp.concatenate(earlier, axis=0), diagonal_blocks(later[0]))
    return both[:64], both[64:] + later[1]


def advance(state, later):
    return fine(dot_nn, state, diagonal_blocks(later[0])) + later[1]


def kernel(
    tokens,
    gain,
    wq,
    wk,
    wv,
    decay_first,
    decay_second,
    channel_decay,
    position_decay,
    extra_decay,
    rate_first,
    rate_second,
    channel_rate,
    own_weight,
    norm_gain,
    start_state,
    wo,
    wi,
    wsig,
    taps,
    conv_gain,
    lin_out,
    conv_out,
    gat_q,
    gat_c,
    raw,
    xn,
    low_d,
    low_r,
    acc,
    q_s,
    k_s,
    v_s,
    decay_s,
    rate_s,
    cum_s,
    rec_s,
    probe_s,
    st1,
    st2,
    st3,
    pre,
    ent,
    sq_s,
    load_sem,
    tok_send,
    tok_recv,
    ici_send,
    ici_recv,
    d2d_send,
    d2d_recv,
    misc_send,
    misc_recv,
):
    z, y, c = (lax.axis_index(n) for n in SP)
    x = lax.axis_index("tp")

    def up(pos, offset):
        return lax.rem(pos + (offset + 4), 4)

    def at_x(o):
        return {"tp": up(x, o)}

    def at_y(o):
        return {"sp_1": up(y, o), "sp_2": 1 - c}

    def at_z(o):
        return {"sp_0": up(z, o), "sp_2": 1 - c}

    def along(o):
        return {"sp_0": up(z, (1 - c) * o), "sp_1": up(y, c * o)}

    sibling = {"sp_2": 1 - c}
    rank = z * 8 + y * 2 + c
    after, before = lax.rem(rank + 1, 32), lax.rem(rank + 31, 32)

    def at_rank(r):
        return {"sp_0": r // 8, "sp_1": lax.rem(r // 2, 4), "sp_2": lax.rem(r, 2)}

    def push(src, dst, send, recv, device):
        copy = pltpu.make_async_remote_copy(
            src_ref=src,
            dst_ref=dst,
            send_sem=send,
            recv_sem=recv,
            device_id=device,
            device_id_type=MESH_IDS,
        )
        copy.start()
        return copy

    def arrived(region, recv):
        pltpu.make_async_copy(region, region, recv).wait()

    loads = [pltpu.make_async_copy(tokens, raw.at[x], load_sem.at[0])]
    for n, (buf, weights) in enumerate(((gat_q, (wq, wk, wv)), (gat_c, (wo, wi, wsig)))):
        for i, (w, first, count, half, at) in enumerate(
            (
                (weights[0], 0, 512, 0, 0),
                (weights[1], 0, 256, 0, 512),
                (weights[1], 256, 256, 1, 0),
                (weights[2], 0, 512, 1, 256),
            )
        ):
            src, dst = w.at[:, pl.ds(first, count)], buf.at[half, rank, :, pl.ds(at, count)]
            loads.append(pltpu.make_async_copy(src, dst, load_sem.at[1 + 4 * n + i]))
    loads.append(pltpu.make_async_copy(decay_first, low_d, load_sem.at[9]))
    loads.append(pltpu.make_async_copy(rate_first, low_r, load_sem.at[10]))
    for load in loads:
        load.start()

    barrier = pltpu.get_barrier_semaphore()
    partners = [f(o) for f in (at_x, at_y, at_z) for o in OFFSETS[1:]] + [along(1), along(-1)]
    partners += [sibling, at_rank(after), at_rank(before)]
    for partner in partners:
        pl.semaphore_signal(barrier, inc=1, device_id=partner, device_id_type=MESH_IDS)
    pl.semaphore_wait(barrier, len(partners))

    loads[0].wait()
    tok_copies = [
        push(raw.at[x], raw.at[x], tok_send.at[0], tok_recv.at[0], at_x(1)),
        push(raw.at[x], raw.at[x], tok_send.at[1], tok_recv.at[1], at_x(-1)),
    ]

    def token_forward():
        left, right = up(x, -1), up(x, 1)
        arrived(raw.at[left], tok_recv.at[0])
        part = raw.at[left, pl.ds(0, 128)]
        tok_copies.append(push(part, part, tok_send.at[2], tok_recv.at[2], at_x(1)))
        arrived(raw.at[right], tok_recv.at[1])
        part = raw.at[right, pl.ds(128, 128)]
        tok_copies.append(push(part, part, tok_send.at[3], tok_recv.at[3], at_x(-1)))

    def token_rest():
        far = up(x, 2)
        arrived(raw.at[far, pl.ds(0, 128)], tok_recv.at[2])
        arrived(raw.at[far, pl.ds(128, 128)], tok_recv.at[3])

    class Gather:
        def __init__(self, which, buf):
            self.g, self.buf = which, buf
            self.first, self.second = 1 - c, c

        def chip(self, ahead, across):
            zz = up(z, (1 - c) * ahead + c * across)
            return zz * 4 + up(y, c * ahead + (1 - c) * across)

        def piece(self, half, ahead, across, part=None):
            blocks = pl.ds(2 * self.chip(ahead, across), 2)
            if part is None:
                return self.buf.at[half, blocks]
            return self.buf.at[half, blocks, pl.ds(64 * part, 64)]

        def recv(self, index):
            return ici_recv.at[self.g * 22 + index]

        def shared(self, index):
            return d2d_recv.at[self.g * 17 + index]

        def send(self, region, direction, index):
            push(region, region, ici_send.at[self.g], self.recv(index), along(direction))

        def share(self, region, index):
            push(region, region, d2d_send.at[self.g], self.shared(index), sibling)

        def start(self):
            self.share(self.buf.at[self.second, rank], 0)
            self.share(self.buf.at[self.first, rank], 1)
            own = self.buf.at[self.first, rank]
            self.send(own, 1, 0)
            self.send(own, -1, 2)

        def start_sibling(self):
            other = rank + 1 - 2 * c
            region = self.buf.at[self.first, other]
            arrived(region, self.shared(0))
            self.send(region, 1, 1)
            self.send(region, -1, 3)
            arrived(self.buf.at[self.second, other], self.shared(1))
            self.spread(0)

        def spread(self, mi):
            region = self.piece(self.second, 0, OFFSETS[mi])
            self.send(region, 1, 6 + 4 * mi)
            self.send(region, -1, 7 + 4 * mi)

        def first_near(self, j):
            offset = (-1, 1)[j]
            for core in range(2):
                block = 2 * self.chip(offset, 0) + (c if core == 0 else 1 - c)
                arrived(self.buf.at[self.first, block], self.recv(2 * j + core))
            self.send(self.piece(self.first, offset, 0, j), -offset, 4 + j)
            self.share(self.piece(self.first, offset, 0), 2 + j)

        def first_far(self):
            for j in range(2):
                arrived(self.piece(self.first, 2, 0, j), self.recv(4 + j))
            self.share(self.piece(self.first, 2, 0), 4)

        def second_start(self, mi):
            arrived(self.piece(self.second, 0, OFFSETS[mi]), self.shared(1 + mi))
            self.spread(mi)

        def second_near(self, mi, j):
            offset = (-1, 1)[j]
            arrived(self.piece(self.second, offset, OFFSETS[mi]), self.recv(6 + 4 * mi + j))
            part = self.piece(self.second, offset, OFFSETS[mi], j)
            self.send(part, -offset, 8 + 4 * mi + j)
            self.share(self.piece(self.second, offset, OFFSETS[mi]), 5 + 3 * mi + j)

        def second_far(self, mi):
            for j in range(2):
                part = self.piece(self.second, 2, OFFSETS[mi], j)
                arrived(part, self.recv(8 + 4 * mi + j))
            self.share(self.piece(self.second, 2, OFFSETS[mi]), 7 + 3 * mi)

        def complete(self, ahead, across):
            if across != 0:
                index = 5 + 3 * OFFSETS.index(ahead) + OFFSETS.index(across) - 1
                arrived(self.piece(self.first, ahead, across), self.shared(index))

        def steps(self):
            def near(mi):
                return [lambda j=j: self.second_near(mi, j) for j in range(2)]

            return [
                [lambda: self.first_near(0), lambda: self.first_near(1)],
                [lambda: self.second_start(1), lambda: self.second_start(2)],
                near(0),
                [self.first_far],
                [lambda: self.second_start(3)],
                near(1),
                near(2),
                [lambda: self.second_far(0)],
                near(3),
                [lambda: self.second_far(1), lambda: self.second_far(2)],
                [lambda: self.second_far(3)],
            ]

        def finish(self):
            arrived(self.buf.at[0, pl.ds(0, 30)], ici_send.at[self.g])
            arrived(self.buf.at[0], d2d_send.at[self.g])

    def run(group):
        for step in group:
            step()

    near = [(a, b) for a in (0, -1, 1) for b in (0, -1, 1)]
    axis_far = [(2, 0), (0, 2)]
    side_far = [(-1, 2), (1, 2), (2, -1), (2, 1)]

    def multiply(gather, chips, first_row, fresh=False):
        rows = pl.ds(first_row, TOK + HALO - first_row)
        for n, (ahead, across) in enumerate(chips):
            gather.complete(ahead, across)
            chip = gather.chip(ahead, across)
            left = xn[chip, rows]
            for half in range(2):
                right = gather.buf[half, pl.ds(chip * 2, 2)].reshape(256, 768)
                part = dot_nn(left, right)
                if fresh and n == 0:
                    acc[half, rows] = part
                else:
                    acc[half, rows] += part

    def projection(i, p):
        at = 512 * i + 128 * p
        return at // 768, slice(at % 768, at % 768 + 128)

    gather_q, gather_c = Gather(0, gat_q), Gather(1, gat_c)
    for load in loads[1:5]:
        load.wait()
    gather_q.start()
    steps_q = gather_q.steps()
    gather_q.start_sibling()
    for n in range(3):
        run(steps_q[n])
    token_forward()
    for n in range(3, 6):
        run(steps_q[n])
    token_rest()

    total = jnp.zeros((TOK, 1), F32)
    for i in range(4):
        wide = raw[i].astype(F32)
        total = total + jnp.sum(wide * wide, axis=1, keepdims=True)
    inverse = lax.rsqrt(total / FEATS + NORM_EPS)
    for i in range(4):
        for j in range(4):
            lanes = slice(256 * j, 256 * (j + 1))
            wide = raw[i, :, lanes].astype(F32) * inverse * gain[:, 1024 * i + 256 * j :][:, :256]
            xn[4 * i + j, pl.ds(HALO, TOK)] = wide.astype(BF16)
    run(steps_q[6])
    run(steps_q[7])
    edge = pl.ds(TOK, HALO)
    halo_copy = push(
        xn.at[:, edge], xn.at[:, pl.ds(0, HALO)], misc_send.at[0], misc_recv.at[0], at_rank(after)
    )

    loads[9].wait()
    loads[10].wait()
    low = jnp.zeros((TOK, 256), F32)
    for i in range(16):
        rows = pl.ds(256 * i, 256)
        both = jnp.concatenate([low_d[rows], low_r[rows]], axis=1)
        low = low + dot_nn(xn[i, pl.ds(HALO, TOK)], both)
    decay_low = jnp.tanh(low[:, :128]).astype(BF16)
    rate_low = low[:, 128:].astype(BF16)
    by_position = jnp.broadcast_to(position_decay[...], (128, TOK)).T
    for p in range(PAIRS):
        lanes = slice(128 * p, 128 * (p + 1))
        logits = channel_decay[:, lanes] + dot_nn(decay_low, decay_second[:, lanes]) + by_position
        heads = [jnp.broadcast_to(extra_decay[h : h + 1], (64, TOK)) for h in (2 * p, 2 * p + 1)]
        extra = jnp.concatenate(heads, axis=0).T
        decay_s[p] = -DECAY_FACTOR * jax.nn.sigmoid(logits) + extra
        rate_s[p] = jax.nn.sigmoid(
            channel_rate[:, lanes] + dot_nn(rate_low, rate_second[:, lanes])
        )
    row, col = iota((TOK, TOK), 0), iota((TOK, TOK), 1)
    summing = (((row // BLK) == (col // BLK)) & (row >= col)).astype(F32).astype(BF16)
    for p in range(PAIRS):
        cum_s[p] = exact_left(summing, decay_s[p])

    multiply(gather_q, near, HALO, True)
    run(steps_q[8])
    multiply(gather_q, axis_far, HALO)
    run(steps_q[9])
    for load in loads[5:9]:
        load.wait()
    gather_c.start()
    multiply(gather_q, side_far, HALO)
    gather_c.start_sibling()
    run(steps_q[10])
    multiply(gather_q, [(2, 2)], HALO)
    body = pl.ds(HALO, TOK)
    for p in range(PAIRS):
        for i, dst in enumerate((q_s, k_s, v_s)):
            half, lanes = projection(i, p)
            dst[p] = acc[half, body, lanes].astype(BF16).astype(F32)

    steps_c = gather_c.steps()

    def held(ref, first, second):
        return ref[first, second, 0].astype(F32), ref[first, second, 1].astype(F32)

    def link(level, p, i):
        return misc_send.at[level + 3 * p + i], misc_recv.at[level + 3 * p + i]

    CORE, YAXIS, ZAXIS, BACK, SQUARES, TOTAL, PREFIX = 1, 16, 28, 40, 44, 47, 51

    def core_send(p):
        part = st1.at[p, c]
        push(part, part, misc_send.at[CORE + p], misc_recv.at[CORE + p], sibling)

    def y_send(p):
        arrived(st1.at[p, 1 - c], misc_recv.at[CORE + p])
        chain, state = compose(held(st1, p, 0), held(st1, p, 1))
        st2[p, y, 0] = chain.astype(BF16)
        st2[p, y, 1] = state.astype(BF16)

        @pl.when(c == 0)
        def _():
            part = st2.at[p, y]
            for i, o in enumerate(OFFSETS[1:]):
                push(part, part, *link(YAXIS, p, i), at_y(o))

    def z_send(p):
        for i, o in enumerate(OFFSETS[1:]):
            arrived(st2.at[p, up(y, -o)], link(YAXIS, p, i)[1])
        eye = (iota((64, 128), 0) == lax.rem(iota((64, 128), 1), 64)).astype(F32)
        prefix = (eye, jnp.zeros((64, 128), F32))
        total_map = held(st2, p, 0)
        for k in range(1, 4):
            prefix = tuple(jnp.where(y >= k, new, old) for new, old in zip(total_map, prefix))
            total_map = compose(total_map, held(st2, p, k))
        for i in range(2):
            pre[p, i] = prefix[i]
            st3[p, z, i] = total_map[i].astype(BF16)
        part = st3.at[p, z]
        for i, o in enumerate(OFFSETS[1:]):
            push(part, part, *link(ZAXIS, p, i), at_z(o))
        push(part, part, misc_send.at[TOTAL + p], misc_recv.at[TOTAL + p], sibling)
        push(pre.at[p], pre.at[p], misc_send.at[PREFIX + p], misc_recv.at[PREFIX + p], sibling)

    def back_send(p):
        for i, o in enumerate(OFFSETS[1:]):
            arrived(st3.at[p, up(z, -o)], link(ZAXIS, p, i)[1])
        arrived(st3.at[p, z], misc_recv.at[TOTAL + p])
        arrived(pre.at[p], misc_recv.at[PREFIX + p])
        state = jnp.concatenate([start_state[2 * p], start_state[2 * p + 1]], axis=1)
        for k in range(3):
            state = jnp.where(z > k, advance(state, held(st3, p, k)), state)
        ent[p] = advance(state, (pre[p, 0], pre[p, 1]))
        push(ent.at[p], ent.at[p], misc_send.at[BACK + p], misc_recv.at[BACK + p], sibling)

    during = {1: steps_c[0], 2: steps_c[1], 3: steps_c[2]}

    def one_pair(p, carry):
        for at, group in during.items():
            pl.when(p == at)(lambda group=group: run(group))
        recalled, probe, state, chain = pair_local(
            q_s[p], k_s[p], v_s[p], decay_s[p], rate_s[p], cum_s[p]
        )
        rec_s[p] = recalled
        probe_s[p] = probe
        st1[p, c, 0] = chain.astype(BF16)
        st1[p, c, 1] = state.astype(BF16)
        core_send(p)
        pl.when(p >= 1)(lambda: y_send(p - 1))
        pl.when((p >= 2) & (c == 1))(lambda: z_send(p - 2))
        return carry

    lax.fori_loop(0, PAIRS, one_pair, 0)
    y_send(3)

    def last_maps(p, carry):
        pl.when(c == 1)(lambda: z_send(p + 2))
        pl.when(c == 0)(lambda: back_send(p))
        return carry

    def last_states(p, carry):
        back_send(p)
        return carry

    lax.fori_loop(0, 1, last_maps, 0)
    run(steps_c[3])
    run(steps_c[4])
    lax.fori_loop(1, 2, last_maps, 0)
    run(steps_c[5])
    arrived(xn.at[:, pl.ds(0, HALO)], misc_recv.at[0])
    halo = xn[:, pl.ds(0, HALO)]
    xn[:, pl.ds(0, HALO)] = jnp.where(rank == 0, jnp.zeros_like(halo), halo)
    run(steps_c[6])

    @pl.when(c == 0)
    def _():
        lax.fori_loop(2, 4, last_states, 0)

    run(steps_c[7])

    def finish_pair(p, carry):
        pl.when(c == 1)(lambda: arrived(ent.at[p], misc_recv.at[BACK + p]))
        state = ent[p]
        state = jnp.where(c == 1, advance(state, held(st1, p, 0)), state)
        recalled = rec_s[p] + fine(dot_nt, probe_s[p], diagonal_blocks(state))
        center = recalled - head_sums(recalled) * (1.0 / 64)
        variance = head_sums(center * center) * (1.0 / 64)
        lanes = pl.ds(pl.multiple_of(128 * p, 128), 128)
        normed = center * lax.rsqrt(variance + GROUP_EPS) * norm_gain[:, lanes]
        own = head_sums(q_s[p] * k_s[p] * own_weight[:, lanes]) * v_s[p]
        lin_out[:, lanes] = (normed + own).astype(BF16)
        return carry

    multiply(gather_c, near, 0, True)
    run(steps_c[8])
    lax.fori_loop(0, PAIRS, finish_pair, 0)

    multiply(gather_c, axis_far, 0)
    run(steps_c[9])
    multiply(gather_c, side_far, 0)
    run(steps_c[10])
    multiply(gather_c, [(2, 2)], 0)
    squares = jnp.zeros((TOK, 128), F32)
    for p in range(PAIRS):
        lanes = slice(128 * p, 128 * (p + 1))
        sums = [acc[projection(i, p)[0], :, projection(i, p)[1]] for i in range(3)]
        outer, inner, signal = (t.astype(BF16).astype(F32) for t in sums)
        mixed = (inner * signal).astype(BF16).astype(F32)
        tap = taps[:, lanes].astype(F32)
        gated = outer[HALO:] * (
            tap[0:1] * pltpu.roll(mixed, 2, 0)[HALO:]
            + tap[1:2] * pltpu.roll(mixed, 1, 0)[HALO:]
            + tap[2:3] * mixed[HALO:]
        )
        q_s[p] = gated
        squares = squares + gated * gated
    column = jnp.broadcast_to(jnp.sum(squares, axis=1, keepdims=True), (TOK, 128))
    sq_s[x] = column.T[:8]
    for i, o in enumerate(OFFSETS[1:]):
        push(sq_s.at[x], sq_s.at[x], misc_send.at[SQUARES + i], misc_recv.at[SQUARES + i], at_x(o))
    gather_q.finish()
    gather_c.finish()
    for copy in tok_copies:
        copy.wait_send()
    halo_copy.wait_send()
    for i, o in enumerate(OFFSETS[1:]):
        arrived(sq_s.at[up(x, -o)], misc_recv.at[SQUARES + i])
    summed = sq_s[0] + sq_s[1] + sq_s[2] + sq_s[3]
    column = jnp.concatenate([summed] * 16, axis=0).T
    scale = lax.rsqrt(column / 2048 + NORM_EPS)
    for p in range(PAIRS):
        lanes = slice(128 * p, 128 * (p + 1))
        conv_out[:, lanes] = (q_s[p] * scale * conv_gain[:, lanes]).astype(BF16)
    for p in range(PAIRS):
        arrived(st1.at[p, c], misc_send.at[CORE + p])

    @pl.when(c == 0)
    def _():
        for p in range(PAIRS):
            arrived(ent.at[p], misc_send.at[BACK + p])
            for i in range(3):
                arrived(st2.at[p, y], link(YAXIS, p, i)[0])

    @pl.when(c == 1)
    def _():
        for p in range(PAIRS):
            arrived(st3.at[p, z], misc_send.at[TOTAL + p])
            arrived(pre.at[p], misc_send.at[PREFIX + p])
            for i in range(3):
                arrived(st3.at[p, z], link(ZAXIS, p, i)[0])

    for i in range(3):
        arrived(sq_s.at[x], misc_send.at[SQUARES + i])


def shards(
    tokens,
    input_norm_gain,
    query_weight,
    key_weight,
    value_weight,
    decay_first_map,
    decay_second_map,
    channel_decay_offset,
    position_decay_offset,
    extra_log_decay,
    rate_first_map,
    rate_second_map,
    channel_rate_offset,
    own_term_weight,
    head_norm_gain,
    starting_state,
    outer_gate_weight,
    inner_gate_weight,
    signal_weight,
    convolution_taps,
    convolution_gain,
):
    far = pl.BlockSpec(memory_space=pl.ANY)
    near = pl.BlockSpec(memory_space=pltpu.VMEM)

    def line(v):
        return v.reshape(1, -1)

    pair = pltpu.VMEM((PAIRS, TOK, 128), F32)
    dma = pltpu.SemaphoreType.DMA
    out = jax.ShapeDtypeStruct((TOK, 512), BF16)
    return pl.pallas_call(
        kernel,
        name="mixer",
        out_shape=(out, out),
        in_specs=[far, near, far, far, far, far, near, near, near, near, far]
        + [near] * 5
        + [far, far, far, near, near],
        out_specs=(near, near),
        scratch_shapes=[
            pltpu.VMEM((2, 32, 128, 768), BF16),
            pltpu.VMEM((2, 32, 128, 768), BF16),
            pltpu.VMEM((4, TOK, 1024), BF16),
            pltpu.VMEM((16, TOK + HALO, 256), BF16),
            pltpu.VMEM((FEATS, 128), BF16),
            pltpu.VMEM((FEATS, 128), BF16),
            pltpu.VMEM((2, TOK + HALO, 768), F32),
        ]
        + [pair] * 8
        + [
            pltpu.VMEM((PAIRS, 2, 2, 64, 128), BF16),
            pltpu.VMEM((PAIRS, 4, 2, 64, 128), BF16),
            pltpu.VMEM((PAIRS, 4, 2, 64, 128), BF16),
            pltpu.VMEM((PAIRS, 2, 64, 128), F32),
            pltpu.VMEM((PAIRS, 64, 128), F32),
            pltpu.VMEM((4, 8, TOK), F32),
            dma((11,)),
            dma((4,)),
            dma((4,)),
            dma((2,)),
            dma((44,)),
            dma((2,)),
            dma((34,)),
            dma((56,)),
            dma((56,)),
        ],
        compiler_params=pltpu.CompilerParams(
            collective_id=0, has_side_effects=True, vmem_limit_bytes=60 * 1024 * 1024
        ),
    )(
        tokens,
        line(input_norm_gain),
        query_weight,
        key_weight,
        value_weight,
        decay_first_map,
        decay_second_map,
        line(channel_decay_offset),
        line(position_decay_offset),
        extra_log_decay.T,
        rate_first_map,
        rate_second_map,
        line(channel_rate_offset),
        line(own_term_weight),
        line(head_norm_gain),
        starting_state,
        outer_gate_weight,
        inner_gate_weight,
        signal_weight,
        convolution_taps,
        line(convolution_gain),
    )


def solution(mesh):
    torus = Mesh(mesh.devices.reshape(4, 4, 2, mesh.shape["tp"]), (*SP, "tp"))
    return jax.shard_map(
        shards,
        mesh=torus,
        in_specs=(
            P(SP, "tp"),
            P(),
            P(SP, "tp"),
            P(SP, "tp"),
            P(SP, "tp"),
            P(),
            P(None, "tp"),
            P("tp"),
            P(SP),
            P(SP, "tp"),
            P(),
            P(None, "tp"),
            P("tp"),
            P("tp"),
            P("tp"),
            P("tp", None, None),
            P(SP, "tp"),
            P(SP, "tp"),
            P(SP, "tp"),
            P(None, "tp"),
            P("tp"),
        ),
        out_specs=(P(SP, "tp"), P(SP, "tp")),
        check_vma=False,
    )
```

time: 103 us -> 90.9 us (0.88)
  Pallas kernels: 98.2 us -> 87.7 us
  local copies, waits for them, and re-layouts: 3.9 us -> 2.42 us
    pallas_call x1, Pallas kernels: 98.2 us -> 87.7 us  [shards(): pl.pallas_call(kernel, name='mixer', out_shape=(out, out), in_specs=[far,...]
    unnamed x7 -> x4, local copies, waits for them, and re-layouts: 3.9 us -> 2.42 us
where the time goes in v2:
time: 90.9 us; the launch traced here: 90.8 us
  Pallas kernels  87.7 us (96%)
  local copies, waits for them, and re-layouts  2.42 us (3%)
    pallas_call x1, Pallas kernels, shards(): pl.pallas_call(kernel, name='mixer', out_shape=(out, out), in_specs=[far,...  87.7 us
    unnamed x4, local copies, waits for them, and re-layouts  2.42 us

profile of v2, /device:TPU:1, one launch (start us, length us, event | category | flops | bytes accessed | tf_op | source)
XLA Modules:
  0.0 90.8 jit_solution(10273410750750233649)
XLA Ops:
  0.6 87.7 %mixer.1 = (bf16[256,512]{1,0:T(8,128)(2,1)}, bf16[256,512]{1,0:T(8,128)(2,1)}) custom-call(bf16[256,1024]{1,0:T(8,128)(2,1)} %tokens.1, f32[1,4096]{1,0:T(1,128)} %bitcast.8, bf16[128,512]{1,0:T(8,128)(2,1)} %wq.1, bf16[128,512]{1,0:T(8,128)(2,1)} %wk.1, bf16[128,512]{1,0:T(8,128)(2,1)} %wv.1, bf16[4096,128]{1,0:T(8,128)(2,1)} %decay_first.1, ...), custom_call_target="tpu_custom_call" | custom-call | tf_op jit(solution)/shard_map/mixer/pallas_call | solution.py:720
  88.3 0.0 copy-start
  88.3 1.7 %copy.25 = bf16[256,512]{1,0:T(8,128)(2,1)} copy(bf16[256,512]{1,0:T(8,128)(2,1)} %get-tuple-element.4) | data formatting | bytes 524288
  90.1 0.0 copy-done
  90.1 0.7 copy.26
Async XLA Ops:
  88.3 1.7 %copy-start = (bf16[256,512]{1,0:T(8,128)(2,1)S(1)}, bf16[256,512]{1,0:T(8,128)(2,1)}, u32[]{:S(2)}) copy-start(bf16[256,512]{1,0:T(8,128)(2,1)} %get-tuple-element.5) | copy-start | bytes 786436

commit v3 on v2

--- a/solution.py
+++ b/solution.py
@@ -171,28 +171,44 @@
 
 def kernel(
     tokens,
-    gain,
+    gain_hbm,
     wq,
     wk,
     wv,
     decay_first,
+    decay_second_hbm,
+    channel_decay_hbm,
+    position_decay_hbm,
+    extra_decay_hbm,
+    rate_first,
+    rate_second_hbm,
+    channel_rate_hbm,
+    own_weight_hbm,
+    norm_gain_hbm,
+    start_state_hbm,
+    wo,
+    wi,
+    wsig,
+    taps_hbm,
+    conv_gain_hbm,
+    lin_hbm,
+    conv_hbm,
+    gain,
     decay_second,
     channel_decay,
     position_decay,
     extra_decay,
-    rate_first,
     rate_second,
     channel_rate,
     own_weight,
     norm_gain,
     start_state,
-    wo,
-    wi,
-    wsig,
     taps,
     conv_gain,
+    small_sem,
     lin_out,
     conv_out,
+    out_sem,
     gat_q,
     gat_c,
     raw,
@@ -213,6 +229,7 @@
     st3,
     pre,
     ent,
+    ent_out,
     sq_s,
     load_sem,
     tok_send,
@@ -278,11 +295,29 @@
             loads.append(pltpu.make_async_copy(src, dst, load_sem.at[1 + 4 * n + i]))
     loads.append(pltpu.make_async_copy(decay_first, low_d, load_sem.at[9]))
     loads.append(pltpu.make_async_copy(rate_first, low_r, load_sem.at[10]))
-    for load in loads:
+    small = [
+        (gain_hbm, gain),
+        (decay_second_hbm, decay_second),
+        (channel_decay_hbm, channel_decay),
+        (position_decay_hbm, position_decay),
+        (extra_decay_hbm, extra_decay),
+        (rate_second_hbm, rate_second),
+        (channel_rate_hbm, channel_rate),
+        (own_weight_hbm, own_weight),
+        (norm_gain_hbm, norm_gain),
+        (start_state_hbm, start_state),
+        (taps_hbm, taps),
+        (conv_gain_hbm, conv_gain),
+    ]
+    small = [
+        pltpu.make_async_copy(src, dst, small_sem.at[i]) for i, (src, dst) in enumerate(small)
+    ]
+    for load in loads + small:
         load.start()
 
     barrier = pltpu.get_barrier_semaphore()
     partners = [f(o) for f in (at_x, at_y, at_z) for o in OFFSETS[1:]] + [along(1), along(-1)]
+    partners += [{"sp_1": up(y, o)} for o in OFFSETS[1:]]
     partners += [sibling, at_rank(after), at_rank(before)]
     for partner in partners:
         pl.semaphore_signal(barrier, inc=1, device_id=partner, device_id_type=MESH_IDS)
@@ -335,9 +370,11 @@
         def share(self, region, index):
             push(region, region, d2d_send.at[self.g], self.shared(index), sibling)
 
-        def start(self):
+        def share_own(self):
             self.share(self.buf.at[self.second, rank], 0)
             self.share(self.buf.at[self.first, rank], 1)
+
+        def start(self):
             own = self.buf.at[self.first, rank]
             self.send(own, 1, 0)
             self.send(own, -1, 2)
@@ -442,6 +479,7 @@
     gather_q, gather_c = Gather(0, gat_q), Gather(1, gat_c)
     for load in loads[1:5]:
         load.wait()
+    gather_q.share_own()
     gather_q.start()
     steps_q = gather_q.steps()
     gather_q.start_sibling()
@@ -452,6 +490,8 @@
         run(steps_q[n])
     token_rest()
 
+    for load in small:
+        load.wait()
     total = jnp.zeros((TOK, 1), F32)
     for i in range(4):
         wide = raw[i].astype(F32)
@@ -493,15 +533,17 @@
     for p in range(PAIRS):
         cum_s[p] = exact_left(summing, decay_s[p])
 
-    multiply(gather_q, near, HALO, True)
+    for load in loads[5:9]:
+        load.wait()
+    gather_c.share_own()
+    multiply(gather_q, near[:6], HALO, True)
     run(steps_q[8])
+    gather_c.start()
+    gather_c.start_sibling()
+    multiply(gather_q, near[6:], HALO)
     multiply(gather_q, axis_far, HALO)
     run(steps_q[9])
-    for load in loads[5:9]:
-        load.wait()
-    gather_c.start()
     multiply(gather_q, side_far, HALO)
-    gather_c.start_sibling()
     run(steps_q[10])
     multiply(gather_q, [(2, 2)], HALO)
     body = pl.ds(HALO, TOK)
@@ -511,14 +553,11 @@
             dst[p] = acc[half, body, lanes].astype(BF16).astype(F32)
 
     steps_c = gather_c.steps()
-
-    def held(ref, first, second):
-        return ref[first, second, 0].astype(F32), ref[first, second, 1].astype(F32)
-
-    def link(level, p, i):
-        return misc_send.at[level + 3 * p + i], misc_recv.at[level + 3 * p + i]
-
-    CORE, YAXIS, ZAXIS, BACK, SQUARES, TOTAL, PREFIX = 1, 16, 28, 40, 44, 47, 51
+    CORE, Y_MAPS, Z_MAPS, TOTAL, PREFIX, ENTER, SQUARES = 1, 5, 9, 13, 14, 15, 19
+    Y_SENT, Z_SENT, BACK_SENT = 24, 28, 32
+
+    def held(ref, *index):
+        return ref[(*index, 0)].astype(F32), ref[(*index, 1)].astype(F32)
 
     def core_send(p):
         part = st1.at[p, c]
@@ -526,46 +565,64 @@
 
     def y_send(p):
         arrived(st1.at[p, 1 - c], misc_recv.at[CORE + p])
-        chain, state = compose(held(st1, p, 0), held(st1, p, 1))
-        st2[p, y, 0] = chain.astype(BF16)
-        st2[p, y, 1] = state.astype(BF16)
-
-        @pl.when(c == 0)
+
+        @pl.when((c == 0) | (p == y))
         def _():
-            part = st2.at[p, y]
-            for i, o in enumerate(OFFSETS[1:]):
-                push(part, part, *link(YAXIS, p, i), at_y(o))
-
-    def z_send(p):
+            maps = compose(held(st1, p, 0), held(st1, p, 1))
+            slot = (1 - c) * (4 + p) + c * y
+            for i in range(2):
+                st2[slot, i] = maps[i].astype(BF16)
+
+        @pl.when((c == 0) & (p != y))
+        def _():
+            push(
+                st2.at[4 + p],
+                st2.at[y],
+                misc_send.at[Y_SENT + p],
+                misc_recv.at[Y_MAPS + y],
+                {"sp_1": p, "sp_2": 1},
+            )
+
+    def z_send():
+        for o in OFFSETS[1:]:
+            arrived(st2.at[up(y, o)], misc_recv.at[Y_MAPS + up(y, o)])
+        total_map = held(st2, 0)
+        for k in range(1, 4):
+            for i in range(2):
+                pre[k - 1, i] = total_map[i]
+            total_map = compose(total_map, held(st2, k))
+        for i in range(2):
+            st3[z, i] = total_map[i].astype(BF16)
+        part = st3.at[z]
         for i, o in enumerate(OFFSETS[1:]):
-            arrived(st2.at[p, up(y, -o)], link(YAXIS, p, i)[1])
-        eye = (iota((64, 128), 0) == lax.rem(iota((64, 128), 1), 64)).astype(F32)
-        prefix = (eye, jnp.zeros((64, 128), F32))
-        total_map = held(st2, p, 0)
-        for k in range(1, 4):
-            prefix = tuple(jnp.where(y >= k, new, old) for new, old in zip(total_map, prefix))
-            total_map = compose(total_map, held(st2, p, k))
-        for i in range(2):
-            pre[p, i] = prefix[i]
-            st3[p, z, i] = total_map[i].astype(BF16)
-        part = st3.at[p, z]
+            push(part, part, misc_send.at[Z_SENT + i], misc_recv.at[Z_MAPS + i], at_z(o))
+        push(part, part, misc_send.at[TOTAL], misc_recv.at[TOTAL], sibling)
+        push(pre, pre, misc_send.at[PREFIX], misc_recv.at[PREFIX], sibling)
+
+    def back_send():
         for i, o in enumerate(OFFSETS[1:]):
-            push(part, part, *link(ZAXIS, p, i), at_z(o))
-        push(part, part, misc_send.at[TOTAL + p], misc_recv.at[TOTAL + p], sibling)
-        push(pre.at[p], pre.at[p], misc_send.at[PREFIX + p], misc_recv.at[PREFIX + p], sibling)
-
-    def back_send(p):
+            arrived(st3.at[up(z, -o)], misc_recv.at[Z_MAPS + i])
+        arrived(st3.at[z], misc_recv.at[TOTAL])
+        state = jnp.concatenate([start_state[2 * y], start_state[2 * y + 1]], axis=1)
+        for k in range(3):
+            state = jnp.where(z > k, advance(state, held(st3, k)), state)
+        arrived(pre, misc_recv.at[PREFIX])
+        ent_out[0] = state.astype(BF16)
+        for k in range(3):
+            ent_out[k + 1] = advance(state, (pre[k, 0], pre[k, 1])).astype(BF16)
+        ent[y] = ent_out[y]
         for i, o in enumerate(OFFSETS[1:]):
-            arrived(st3.at[p, up(z, -o)], link(ZAXIS, p, i)[1])
-        arrived(st3.at[p, z], misc_recv.at[TOTAL + p])
-        arrived(pre.at[p], misc_recv.at[PREFIX + p])
-        state = jnp.concatenate([start_state[2 * p], start_state[2 * p + 1]], axis=1)
-        for k in range(3):
-            state = jnp.where(z > k, advance(state, held(st3, p, k)), state)
-        ent[p] = advance(state, (pre[p, 0], pre[p, 1]))
-        push(ent.at[p], ent.at[p], misc_send.at[BACK + p], misc_recv.at[BACK + p], sibling)
-
-    during = {1: steps_c[0], 2: steps_c[1], 3: steps_c[2]}
+            for core in range(2):
+                push(
+                    ent_out.at[up(y, o)],
+                    ent.at[y],
+                    misc_send.at[BACK_SENT + 2 * i + core],
+                    misc_recv.at[ENTER + y],
+                    {"sp_1": up(y, o), "sp_2": core},
+                )
+        push(ent_out.at[y], ent.at[y], misc_send.at[BACK_SENT + 6], misc_recv.at[ENTER + y], sibling)
+
+    during = dict(enumerate(steps_c[:4]))
 
     def one_pair(p, carry):
         for at, group in during.items():
@@ -579,40 +636,24 @@
         st1[p, c, 1] = state.astype(BF16)
         core_send(p)
         pl.when(p >= 1)(lambda: y_send(p - 1))
-        pl.when((p >= 2) & (c == 1))(lambda: z_send(p - 2))
         return carry
 
     lax.fori_loop(0, PAIRS, one_pair, 0)
     y_send(3)
 
-    def last_maps(p, carry):
-        pl.when(c == 1)(lambda: z_send(p + 2))
-        pl.when(c == 0)(lambda: back_send(p))
-        return carry
-
-    def last_states(p, carry):
-        back_send(p)
-        return carry
-
-    lax.fori_loop(0, 1, last_maps, 0)
-    run(steps_c[3])
     run(steps_c[4])
-    lax.fori_loop(1, 2, last_maps, 0)
     run(steps_c[5])
+    pl.when(c == 1)(z_send)
+    run(steps_c[6])
+    pl.when(c == 0)(back_send)
+    run(steps_c[7])
     arrived(xn.at[:, pl.ds(0, HALO)], misc_recv.at[0])
     halo = xn[:, pl.ds(0, HALO)]
     xn[:, pl.ds(0, HALO)] = jnp.where(rank == 0, jnp.zeros_like(halo), halo)
-    run(steps_c[6])
-
-    @pl.when(c == 0)
-    def _():
-        lax.fori_loop(2, 4, last_states, 0)
-
-    run(steps_c[7])
 
     def finish_pair(p, carry):
-        pl.when(c == 1)(lambda: arrived(ent.at[p], misc_recv.at[BACK + p]))
-        state = ent[p]
+        pl.when((c == 1) | (p != y))(lambda: arrived(ent.at[p], misc_recv.at[ENTER + p]))
+        state = ent[p].astype(F32)
         state = jnp.where(c == 1, advance(state, held(st1, p, 0)), state)
         recalled = rec_s[p] + fine(dot_nt, probe_s[p], diagonal_blocks(state))
         center = recalled - head_sums(recalled) * (1.0 / 64)
@@ -623,10 +664,13 @@
         lin_out[:, lanes] = (normed + own).astype(BF16)
         return carry
 
-    multiply(gather_c, near, 0, True)
+    multiply(gather_c, near[:5], 0, True)
     run(steps_c[8])
+    multiply(gather_c, near[5:], 0)
     lax.fori_loop(0, PAIRS, finish_pair, 0)
 
+    lin_copy = pltpu.make_async_copy(lin_out, lin_hbm, out_sem.at[0])
+    lin_copy.start()
     multiply(gather_c, axis_far, 0)
     run(steps_c[9])
     multiply(gather_c, side_far, 0)
@@ -663,26 +707,29 @@
     for p in range(PAIRS):
         lanes = slice(128 * p, 128 * (p + 1))
         conv_out[:, lanes] = (q_s[p] * scale * conv_gain[:, lanes]).astype(BF16)
+    conv_copy = pltpu.make_async_copy(conv_out, conv_hbm, out_sem.at[1])
+    conv_copy.start()
     for p in range(PAIRS):
         arrived(st1.at[p, c], misc_send.at[CORE + p])
 
     @pl.when(c == 0)
     def _():
         for p in range(PAIRS):
-            arrived(ent.at[p], misc_send.at[BACK + p])
-            for i in range(3):
-                arrived(st2.at[p, y], link(YAXIS, p, i)[0])
+            pl.when(y != p)(lambda p=p: arrived(st2.at[4 + p], misc_send.at[Y_SENT + p]))
+        for i in range(7):
+            arrived(ent_out.at[0], misc_send.at[BACK_SENT + i])
 
     @pl.when(c == 1)
     def _():
-        for p in range(PAIRS):
-            arrived(st3.at[p, z], misc_send.at[TOTAL + p])
-            arrived(pre.at[p], misc_send.at[PREFIX + p])
-            for i in range(3):
-                arrived(st3.at[p, z], link(ZAXIS, p, i)[0])
+        for i in range(3):
+            arrived(st3.at[z], misc_send.at[Z_SENT + i])
+        arrived(st3.at[z], misc_send.at[TOTAL])
+        arrived(pre, misc_send.at[PREFIX])
 
     for i in range(3):
         arrived(sq_s.at[x], misc_send.at[SQUARES + i])
+    lin_copy.wait()
+    conv_copy.wait()
 
 
 def shards(
@@ -709,7 +756,6 @@
     convolution_gain,
 ):
     far = pl.BlockSpec(memory_space=pl.ANY)
-    near = pl.BlockSpec(memory_space=pltpu.VMEM)
 
     def line(v):
         return v.reshape(1, -1)
@@ -721,11 +767,25 @@
         kernel,
         name="mixer",
         out_shape=(out, out),
-        in_specs=[far, near, far, far, far, far, near, near, near, near, far]
-        + [near] * 5
-        + [far, far, far, near, near],
-        out_specs=(near, near),
+        in_specs=[far] * 21,
+        out_specs=(far, far),
         scratch_shapes=[
+            pltpu.VMEM((1, FEATS), F32),
+            pltpu.VMEM((128, 512), BF16),
+            pltpu.VMEM((1, 512), F32),
+            pltpu.VMEM((1, TOK), F32),
+            pltpu.VMEM((8, TOK), F32),
+            pltpu.VMEM((128, 512), BF16),
+            pltpu.VMEM((1, 512), F32),
+            pltpu.VMEM((1, 512), F32),
+            pltpu.VMEM((1, 512), F32),
+            pltpu.VMEM((8, 64, 64), F32),
+            pltpu.VMEM((3, 512), BF16),
+            pltpu.VMEM((1, 512), F32),
+            dma((12,)),
+            pltpu.VMEM((TOK, 512), BF16),
+            pltpu.VMEM((TOK, 512), BF16),
+            dma((2,)),
             pltpu.VMEM((2, 32, 128, 768), BF16),
             pltpu.VMEM((2, 32, 128, 768), BF16),
             pltpu.VMEM((4, TOK, 1024), BF16),
@@ -737,10 +797,11 @@
         + [pair] * 8
         + [
             pltpu.VMEM((PAIRS, 2, 2, 64, 128), BF16),
-            pltpu.VMEM((PAIRS, 4, 2, 64, 128), BF16),
-            pltpu.VMEM((PAIRS, 4, 2, 64, 128), BF16),
-            pltpu.VMEM((PAIRS, 2, 64, 128), F32),
-            pltpu.VMEM((PAIRS, 64, 128), F32),
+            pltpu.VMEM((8, 2, 64, 128), BF16),
+            pltpu.VMEM((4, 2, 64, 128), BF16),
+            pltpu.VMEM((3, 2, 64, 128), F32),
+            pltpu.VMEM((PAIRS, 64, 128), BF16),
+            pltpu.VMEM((4, 64, 128), BF16),
             pltpu.VMEM((4, 8, TOK), F32),
             dma((11,)),
             dma((4,)),

time: 90.9 us -> 88.6 us (0.975)
  Pallas kernels: 87.7 us -> 84.7 us
    pallas_call x1, Pallas kernels: 87.7 us -> 84.7 us  [shards(): pl.pallas_call(kernel, name='mixer', out_shape=(out, out), in_specs=[far]...]
where the time goes in v3:
time: 88.6 us; the launch traced here: 87.8 us
  Pallas kernels  84.7 us (96%)
  local copies, waits for them, and re-layouts  2.42 us (3%)
    pallas_call x1, Pallas kernels, shards(): pl.pallas_call(kernel, name='mixer', out_shape=(out, out), in_specs=[far]...  84.7 us
    unnamed x4, local copies, waits for them, and re-layouts  2.42 us

profile of v3, /device:TPU:1, one launch (start us, length us, event | category | flops | bytes accessed | tf_op | source)
XLA Modules:
  0.0 87.8 jit_solution(8039758127450725153)
XLA Ops:
  0.6 84.7 %mixer.1 = (bf16[256,512]{1,0:T(8,128)(2,1)}, bf16[256,512]{1,0:T(8,128)(2,1)}) custom-call(bf16[256,1024]{1,0:T(8,128)(2,1)} %tokens.1, f32[1,4096]{1,0:T(1,128)} %bitcast.8, bf16[128,512]{1,0:T(8,128)(2,1)} %wq.1, bf16[128,512]{1,0:T(8,128)(2,1)} %wk.1, bf16[128,512]{1,0:T(8,128)(2,1)} %wv.1, bf16[4096,128]{1,0:T(8,128)(2,1)} %decay_first.1, ...), custom_call_target="tpu_custom_call" | custom-call | tf_op jit(solution)/shard_map/mixer/pallas_call | solution.py:766
  85.4 0.0 copy-start
  85.4 1.7 %copy.25 = bf16[256,512]{1,0:T(8,128)(2,1)} copy(bf16[256,512]{1,0:T(8,128)(2,1)} %get-tuple-element.4) | data formatting | bytes 524288
  87.1 0.0 copy-done
  87.1 0.7 copy.26
Async XLA Ops:
  85.4 1.7 %copy-start = (bf16[256,512]{1,0:T(8,128)(2,1)S(1)}, bf16[256,512]{1,0:T(8,128)(2,1)}, u32[]{:S(2)}) copy-start(bf16[256,512]{1,0:T(8,128)(2,1)} %get-tuple-element.5) | copy-start | bytes 786436

commit v4 on v3

--- a/solution.py
+++ b/solution.py
@@ -352,11 +352,14 @@
             zz = up(z, (1 - c) * ahead + c * across)
             return zz * 4 + up(y, c * ahead + (1 - c) * across)
 
-        def piece(self, half, ahead, across, part=None):
+        def piece(self, half, ahead, across, part=None, cut=64):
             blocks = pl.ds(2 * self.chip(ahead, across), 2)
             if part is None:
                 return self.buf.at[half, blocks]
-            return self.buf.at[half, blocks, pl.ds(64 * part, 64)]
+            return self.buf.at[half, blocks, pl.ds(cut * part, (cut, 128 - cut)[part])]
+
+        def cut(self, mi):
+            return 48 if self.g == 1 and mi == 1 else 64
 
         def recv(self, index):
             return ici_recv.at[self.g * 22 + index]
@@ -413,13 +416,13 @@
         def second_near(self, mi, j):
             offset = (-1, 1)[j]
             arrived(self.piece(self.second, offset, OFFSETS[mi]), self.recv(6 + 4 * mi + j))
-            part = self.piece(self.second, offset, OFFSETS[mi], j)
+            part = self.piece(self.second, offset, OFFSETS[mi], j, self.cut(mi))
             self.send(part, -offset, 8 + 4 * mi + j)
             self.share(self.piece(self.second, offset, OFFSETS[mi]), 5 + 3 * mi + j)
 
         def second_far(self, mi):
             for j in range(2):
-                part = self.piece(self.second, 2, OFFSETS[mi], j)
+                part = self.piece(self.second, 2, OFFSETS[mi], j, self.cut(mi))
                 arrived(part, self.recv(8 + 4 * mi + j))
             self.share(self.piece(self.second, 2, OFFSETS[mi]), 7 + 3 * mi)
 
@@ -543,8 +546,8 @@
     multiply(gather_q, near[6:], HALO)
     multiply(gather_q, axis_far, HALO)
     run(steps_q[9])
+    run(steps_q[10])
     multiply(gather_q, side_far, HALO)
-    run(steps_q[10])
     multiply(gather_q, [(2, 2)], HALO)
     body = pl.ds(HALO, TOK)
     for p in range(PAIRS):
@@ -673,8 +676,8 @@
     lin_copy.start()
     multiply(gather_c, axis_far, 0)
     run(steps_c[9])
+    run(steps_c[10])
     multiply(gather_c, side_far, 0)
-    run(steps_c[10])
     multiply(gather_c, [(2, 2)], 0)
     squares = jnp.zeros((TOK, 128), F32)
     for p in range(PAIRS):

time: 88.6 us -> 87.8 us (level)
  no operation moved by 1% of the time
where the time goes in v4:
time: 87.8 us; the launch traced here: 87.7 us
  Pallas kernels  84.6 us (96%)
  local copies, waits for them, and re-layouts  2.42 us (3%)
    pallas_call x1, Pallas kernels, shards(): pl.pallas_call(kernel, name='mixer', out_shape=(out, out), in_specs=[far]...  84.6 us
    unnamed x4, local copies, waits for them, and re-layouts  2.42 us

profile of v4, /device:TPU:1, one launch (start us, length us, event | category | flops | bytes accessed | tf_op | source)
XLA Modules:
  0.0 87.7 jit_solution(14266926026828674850)
XLA Ops:
  0.6 84.6 %mixer.1 = (bf16[256,512]{1,0:T(8,128)(2,1)}, bf16[256,512]{1,0:T(8,128)(2,1)}) custom-call(bf16[256,1024]{1,0:T(8,128)(2,1)} %tokens.1, f32[1,4096]{1,0:T(1,128)} %bitcast.8, bf16[128,512]{1,0:T(8,128)(2,1)} %wq.1, bf16[128,512]{1,0:T(8,128)(2,1)} %wk.1, bf16[128,512]{1,0:T(8,128)(2,1)} %wv.1, bf16[4096,128]{1,0:T(8,128)(2,1)} %decay_first.1, ...), custom_call_target="tpu_custom_call" | custom-call | tf_op jit(solution)/shard_map/mixer/pallas_call | solution.py:769
  85.2 0.0 copy-start
  85.3 1.7 %copy.25 = bf16[256,512]{1,0:T(8,128)(2,1)} copy(bf16[256,512]{1,0:T(8,128)(2,1)} %get-tuple-element.4) | data formatting | bytes 524288
  87.0 0.0 copy-done
  87.0 0.7 copy.26
Async XLA Ops:
  85.2 1.7 %copy-start = (bf16[256,512]{1,0:T(8,128)(2,1)S(1)}, bf16[256,512]{1,0:T(8,128)(2,1)}, u32[]{:S(2)}) copy-start(bf16[256,512]{1,0:T(8,128)(2,1)} %get-tuple-element.5) | copy-start | bytes 786436

commit v5 on v4

--- a/solution.py
+++ b/solution.py
@@ -190,9 +190,9 @@
     wi,
     wsig,
     taps_hbm,
-    conv_gain_hbm,
     lin_hbm,
-    conv_hbm,
+    gated_hbm,
+    total_hbm,
     gain,
     decay_second,
     channel_decay,
@@ -204,10 +204,9 @@
     norm_gain,
     start_state,
     taps,
-    conv_gain,
     small_sem,
     lin_out,
-    conv_out,
+    total_out,
     out_sem,
     gat_q,
     gat_c,
@@ -307,7 +306,6 @@
         (norm_gain_hbm, norm_gain),
         (start_state_hbm, start_state),
         (taps_hbm, taps),
-        (conv_gain_hbm, conv_gain),
     ]
     small = [
         pltpu.make_async_copy(src, dst, small_sem.at[i]) for i, (src, dst) in enumerate(small)
@@ -365,7 +363,7 @@
             return ici_recv.at[self.g * 22 + index]
 
         def shared(self, index):
-            return d2d_recv.at[self.g * 17 + index]
+            return d2d_recv.at[self.g * 18 + index]
 
         def send(self, region, direction, index):
             push(region, region, ici_send.at[self.g], self.recv(index), along(direction))
@@ -424,10 +422,16 @@
             for j in range(2):
                 part = self.piece(self.second, 2, OFFSETS[mi], j, self.cut(mi))
                 arrived(part, self.recv(8 + 4 * mi + j))
-            self.share(self.piece(self.second, 2, OFFSETS[mi]), 7 + 3 * mi)
+                if mi == 3:
+                    self.share(part, 16 + j)
+            if mi < 3:
+                self.share(self.piece(self.second, 2, OFFSETS[mi]), 7 + 3 * mi)
 
         def complete(self, ahead, across):
-            if across != 0:
+            if (ahead, across) == (2, 2):
+                for j in range(2):
+                    arrived(self.piece(self.first, 2, 2, j), self.shared(16 + j))
+            elif across != 0:
                 index = 5 + 3 * OFFSETS.index(ahead) + OFFSETS.index(across) - 1
                 arrived(self.piece(self.first, ahead, across), self.shared(index))
 
@@ -445,7 +449,8 @@
                 near(2),
                 [lambda: self.second_far(0)],
                 near(3),
-                [lambda: self.second_far(1), lambda: self.second_far(2)],
+                [lambda: self.second_far(1)],
+                [lambda: self.second_far(2)],
                 [lambda: self.second_far(3)],
             ]
 
@@ -547,7 +552,9 @@
     multiply(gather_q, axis_far, HALO)
     run(steps_q[9])
     run(steps_q[10])
-    multiply(gather_q, side_far, HALO)
+    multiply(gather_q, side_far[2:], HALO)
+    run(steps_q[11])
+    multiply(gather_q, side_far[:2], HALO)
     multiply(gather_q, [(2, 2)], HALO)
     body = pl.ds(HALO, TOK)
     for p in range(PAIRS):
@@ -667,17 +674,18 @@
         lin_out[:, lanes] = (normed + own).astype(BF16)
         return carry
 
-    multiply(gather_c, near[:5], 0, True)
+    multiply(gather_c, near, 0, True)
+    lax.fori_loop(0, 2, finish_pair, 0)
     run(steps_c[8])
-    multiply(gather_c, near[5:], 0)
-    lax.fori_loop(0, PAIRS, finish_pair, 0)
-
+    lax.fori_loop(2, PAIRS, finish_pair, 0)
     lin_copy = pltpu.make_async_copy(lin_out, lin_hbm, out_sem.at[0])
     lin_copy.start()
     multiply(gather_c, axis_far, 0)
     run(steps_c[9])
     run(steps_c[10])
-    multiply(gather_c, side_far, 0)
+    multiply(gather_c, side_far[2:], 0)
+    run(steps_c[11])
+    multiply(gather_c, side_far[:2], 0)
     multiply(gather_c, [(2, 2)], 0)
     squares = jnp.zeros((TOK, 128), F32)
     for p in range(PAIRS):
@@ -694,9 +702,11 @@
         q_s[p] = gated
         squares = squares + gated * gated
     column = jnp.broadcast_to(jnp.sum(squares, axis=1, keepdims=True), (TOK, 128))
+    gated_copy = pltpu.make_async_copy(q_s, gated_hbm, out_sem.at[2])
     sq_s[x] = column.T[:8]
     for i, o in enumerate(OFFSETS[1:]):
         push(sq_s.at[x], sq_s.at[x], misc_send.at[SQUARES + i], misc_recv.at[SQUARES + i], at_x(o))
+    gated_copy.start()
     gather_q.finish()
     gather_c.finish()
     for copy in tok_copies:
@@ -704,14 +714,9 @@
     halo_copy.wait_send()
     for i, o in enumerate(OFFSETS[1:]):
         arrived(sq_s.at[up(x, -o)], misc_recv.at[SQUARES + i])
-    summed = sq_s[0] + sq_s[1] + sq_s[2] + sq_s[3]
-    column = jnp.concatenate([summed] * 16, axis=0).T
-    scale = lax.rsqrt(column / 2048 + NORM_EPS)
-    for p in range(PAIRS):
-        lanes = slice(128 * p, 128 * (p + 1))
-        conv_out[:, lanes] = (q_s[p] * scale * conv_gain[:, lanes]).astype(BF16)
-    conv_copy = pltpu.make_async_copy(conv_out, conv_hbm, out_sem.at[1])
-    conv_copy.start()
+    total_out[...] = sq_s[0] + sq_s[1] + sq_s[2] + sq_s[3]
+    total_copy = pltpu.make_async_copy(total_out, total_hbm, out_sem.at[1])
+    total_copy.start()
     for p in range(PAIRS):
         arrived(st1.at[p, c], misc_send.at[CORE + p])
 
@@ -732,7 +737,17 @@
     for i in range(3):
         arrived(sq_s.at[x], misc_send.at[SQUARES + i])
     lin_copy.wait()
-    conv_copy.wait()
+    gated_copy.wait()
+    total_copy.wait()
+
+
+def finish(linear, gated, total, gain, lin_out, conv_out):
+    lin_out[...] = linear[...]
+    column = jnp.concatenate([total[...]] * 16, axis=0).T
+    scale = lax.rsqrt(column / 2048 + NORM_EPS)
+    for p in range(PAIRS):
+        lanes = slice(128 * p, 128 * (p + 1))
+        conv_out[:, lanes] = (gated[p] * scale * gain[:, lanes]).astype(BF16)
 
 
 def shards(
@@ -766,12 +781,16 @@
     pair = pltpu.VMEM((PAIRS, TOK, 128), F32)
     dma = pltpu.SemaphoreType.DMA
     out = jax.ShapeDtypeStruct((TOK, 512), BF16)
-    return pl.pallas_call(
+    linear, gated, total = pl.pallas_call(
         kernel,
         name="mixer",
-        out_shape=(out, out),
-        in_specs=[far] * 21,
-        out_specs=(far, far),
+        out_shape=(
+            out,
+            jax.ShapeDtypeStruct((PAIRS, TOK, 128), F32),
+            jax.ShapeDtypeStruct((8, TOK), F32),
+        ),
+        in_specs=[far] * 20,
+        out_specs=(far, far, far),
         scratch_shapes=[
             pltpu.VMEM((1, FEATS), F32),
             pltpu.VMEM((128, 512), BF16),
@@ -784,11 +803,10 @@
             pltpu.VMEM((1, 512), F32),
             pltpu.VMEM((8, 64, 64), F32),
             pltpu.VMEM((3, 512), BF16),
-            pltpu.VMEM((1, 512), F32),
-            dma((12,)),
+            dma((11,)),
             pltpu.VMEM((TOK, 512), BF16),
-            pltpu.VMEM((TOK, 512), BF16),
-            dma((2,)),
+            pltpu.VMEM((8, TOK), F32),
+            dma((3,)),
             pltpu.VMEM((2, 32, 128, 768), BF16),
             pltpu.VMEM((2, 32, 128, 768), BF16),
             pltpu.VMEM((4, TOK, 1024), BF16),
@@ -812,7 +830,7 @@
             dma((2,)),
             dma((44,)),
             dma((2,)),
-            dma((34,)),
+            dma((36,)),
             dma((56,)),
             dma((56,)),
         ],
@@ -840,7 +858,9 @@
         inner_gate_weight,
         signal_weight,
         convolution_taps,
-        line(convolution_gain),
+    )
+    return pl.pallas_call(finish, name="finish", out_shape=(out, out))(
+        linear, gated, total, line(convolution_gain)
     )
 
 

time: 87.8 us -> 86.6 us (0.986)
  local copies, waits for them, and re-layouts: 2.42 us -> 0 us
  Pallas kernels: 84.6 us -> 85.9 us
    unnamed x4 -> x0, local copies, waits for them, and re-layouts: 2.42 us -> none
    pallas_call x1 -> x2, Pallas kernels: 84.6 us -> 85.9 us  [the longest x1 83.9 us: shards(): pl.pallas_call(kernel, name='mixer', out_shape=(out, jax.ShapeDtypeStruct...]
where the time goes in v5:
time: 86.6 us; the launch traced here: 86.5 us
  Pallas kernels  85.9 us (99%)
    pallas_call x1, Pallas kernels, shards(): pl.pallas_call(kernel, name='mixer', out_shape=(out, jax.ShapeDtypeStruct...  83.9 us
    pallas_call x1, Pallas kernels, shards(): pl.pallas_call(finish, name='finish', out_shape=(out, out))  2 us

profile of v5, /device:TPU:1, one launch (start us, length us, event | category | flops | bytes accessed | tf_op | source)
XLA Modules:
  0.0 86.5 jit_solution(13449403027658945988)
XLA Ops:
  0.6 83.9 %mixer.1 = (bf16[256,512]{1,0:T(8,128)(2,1)}, f32[4,256,128]{2,1,0:T(8,128)}, f32[8,256]{1,0:T(8,128)}) custom-call(bf16[256,1024]{1,0:T(8,128)(2,1)} %tokens.1, f32[1,4096]{1,0:T(1,128)} %bitcast.8, bf16[128,512]{1,0:T(8,128)(2,1)} %wq.1, bf16[128,512]{1,0:T(8,128)(2,1)} %wk.1, bf16[128,512]{1,0:T(8,128)(2,1)} %wv.1, bf16[4096,128]{1,0:T(8,128)(2,1)} %decay_first.1, ...), custom_call_target="tpu_custom_call" | custom-call | tf_op jit(solution)/shard_map/mixer/pallas_call | solution.py:784
  84.5 2.0 %finish.1 = (bf16[256,512]{1,0:T(8,128)(2,1)}, bf16[256,512]{1,0:T(8,128)(2,1)}) custom-call(bf16[256,512]{1,0:T(8,128)(2,1)} %get-tuple-element.5.linear, f32[4,256,128]{2,1,0:T(8,128)} %get-tuple-element.6.gated, f32[8,256]{1,0:T(8,128)} %get-tuple-element.7.total, f32[1,512]{1,0:T(1,128)} %bitcast.14), custom_call_target="tpu_custom_call" | custom-call | tf_op jit(solution)/shard_map/finish/pallas_call | solution.py:862

commit v6 on v5

--- a/solution.py
+++ b/solution.py
@@ -86,10 +86,12 @@
     later, earlier = iota((BLK, 128), 0), lax.rem(iota((BLK, 128), 1), BLK)
     strict, inclusive = later > earlier, later >= earlier
     unit = k * lax.rsqrt(head_sums(k * k) + KEY_EPS)
-    grow = jnp.exp(-cum)
-    a = -unit * jnp.exp(cum - decay)
+    middles = [cum[t.start + BLK // 2 - 1 : t.start + BLK // 2, :] for t in rows]
+    middle = jnp.concatenate([jnp.broadcast_to(t, (BLK, 128)) for t in middles], axis=0)
+    grow = jnp.exp(middle - cum)
+    a = -unit * jnp.exp(cum - decay - middle)
     b = unit * rate
-    r = q * jnp.exp(cum)
+    r = q * jnp.exp(cum - middle)
     a16, r16, v16 = a.astype(BF16), r.astype(BF16), v.astype(BF16)
     b16, k16 = (b * grow).astype(BF16), (k * grow).astype(BF16)
     grams = [
@@ -137,17 +139,19 @@
         last = cum[BLK * (n + 1) - 1 : BLK * (n + 1), :]
         fade = jnp.exp(last - cum[rows[n]])
         b_end, k_end = b[rows[n]] * fade, k[rows[n]] * fade
-        solved = jnp.concatenate([keys_solved[n], free_solved[n]], axis=1)
+        solved = [keys_solved[n] * jnp.exp(middles[n]), free_solved[n]]
+        solved = jnp.concatenate(solved, axis=1)
         both = fine(dot_tn, solved, b_end)
         step = jnp.where(same_head(), both[:128], 0.0)
         steps.append(step + jnp.where(eye, jnp.broadcast_to(jnp.exp(last), (128, 128)), 0.0))
         gain = both[128:] + fine(dot_tn, v[rows[n]], k_end)
         gains.append(jnp.where(same_head(), gain, 0.0))
     state, chain = gains[0], steps[0]
-    recalled, probes = [read[0][:, 128:]], [r[rows[0]] + read[0][:, :128]]
+    asked = [(r[rows[n]] + read[n][:, :128]) * jnp.exp(middles[n]) for n in chunks]
+    recalled, probes = [read[0][:, 128:]], [asked[0]]
     for n in chunks[1:]:
         carried = jnp.concatenate([state, chain], axis=0)
-        both = fine(dot_nt, r[rows[n]] + read[n][:, :128], carried)
+        both = fine(dot_nt, asked[n], carried)
         recalled.append(read[n][:, 128:] + both[:, :128])
         probes.append(both[:, 128:])
         both = fine(dot_nn, carried, steps[n])

time: 86.6 us -> 86.6 us (level)
  no operation moved by 1% of the time
where the time goes in v6:
time: 86.6 us; the launch traced here: 86.5 us
  Pallas kernels  85.9 us (99%)
    pallas_call x1, Pallas kernels, shards(): pl.pallas_call(kernel, name='mixer', out_shape=(out, jax.ShapeDtypeStruct...  83.9 us
    pallas_call x1, Pallas kernels, shards(): pl.pallas_call(finish, name='finish', out_shape=(out, out))  2 us

profile of v6, /device:TPU:1, one launch (start us, length us, event | category | flops | bytes accessed | tf_op | source)
XLA Modules:
  0.0 86.5 jit_solution(1502776006573828032)
XLA Ops:
  0.6 83.9 %mixer.1 = (bf16[256,512]{1,0:T(8,128)(2,1)}, f32[4,256,128]{2,1,0:T(8,128)}, f32[8,256]{1,0:T(8,128)}) custom-call(bf16[256,1024]{1,0:T(8,128)(2,1)} %tokens.1, f32[1,4096]{1,0:T(1,128)} %bitcast.8, bf16[128,512]{1,0:T(8,128)(2,1)} %wq.1, bf16[128,512]{1,0:T(8,128)(2,1)} %wk.1, bf16[128,512]{1,0:T(8,128)(2,1)} %wv.1, bf16[4096,128]{1,0:T(8,128)(2,1)} %decay_first.1, ...), custom_call_target="tpu_custom_call" | custom-call | tf_op jit(solution)/shard_map/mixer/pallas_call | solution.py:788
  84.5 2.0 %finish.1 = (bf16[256,512]{1,0:T(8,128)(2,1)}, bf16[256,512]{1,0:T(8,128)(2,1)}) custom-call(bf16[256,512]{1,0:T(8,128)(2,1)} %get-tuple-element.5.linear, f32[4,256,128]{2,1,0:T(8,128)} %get-tuple-element.6.gated, f32[8,256]{1,0:T(8,128)} %get-tuple-element.7.total, f32[1,512]{1,0:T(1,128)} %bitcast.14), custom_call_target="tpu_custom_call" | custom-call | tf_op jit(solution)/shard_map/finish/pallas_call | solution.py:866

commit v7 on v6

--- a/solution.py
+++ b/solution.py
@@ -318,9 +318,7 @@
         load.start()
 
     barrier = pltpu.get_barrier_semaphore()
-    partners = [f(o) for f in (at_x, at_y, at_z) for o in OFFSETS[1:]] + [along(1), along(-1)]
-    partners += [{"sp_1": up(y, o)} for o in OFFSETS[1:]]
-    partners += [sibling, at_rank(after), at_rank(before)]
+    partners = [at_x(1), at_x(-1), along(1), along(-1), sibling]
     for partner in partners:
         pl.semaphore_signal(barrier, inc=1, device_id=partner, device_id_type=MESH_IDS)
     pl.semaphore_wait(barrier, len(partners))

time: 86.6 us -> 85 us (0.982)
  Pallas kernels: 85.9 us -> 83.9 us
    pallas_call x1, Pallas kernels: 83.9 us -> 81.9 us  [shards(): pl.pallas_call(kernel, name='mixer', out_shape=(out, jax.ShapeDtypeStruct...]
where the time goes in v7:
time: 85 us; the launch traced here: 84.6 us
  Pallas kernels  83.9 us (99%)
    pallas_call x1, Pallas kernels, shards(): pl.pallas_call(kernel, name='mixer', out_shape=(out, jax.ShapeDtypeStruct...  81.9 us
    pallas_call x1, Pallas kernels, shards(): pl.pallas_call(finish, name='finish', out_shape=(out, out))  2 us

profile of v7, /device:TPU:1, one launch (start us, length us, event | category | flops | bytes accessed | tf_op | source)
XLA Modules:
  0.0 84.6 jit_solution(2781776806377413551)
XLA Ops:
  0.6 81.9 %mixer.1 = (bf16[256,512]{1,0:T(8,128)(2,1)}, f32[4,256,128]{2,1,0:T(8,128)}, f32[8,256]{1,0:T(8,128)}) custom-call(bf16[256,1024]{1,0:T(8,128)(2,1)} %tokens.1, f32[1,4096]{1,0:T(1,128)} %bitcast.8, bf16[128,512]{1,0:T(8,128)(2,1)} %wq.1, bf16[128,512]{1,0:T(8,128)(2,1)} %wk.1, bf16[128,512]{1,0:T(8,128)(2,1)} %wv.1, bf16[4096,128]{1,0:T(8,128)(2,1)} %decay_first.1, ...), custom_call_target="tpu_custom_call" | custom-call | tf_op jit(solution)/shard_map/mixer/pallas_call | solution.py:786
  82.6 2.0 %finish.1 = (bf16[256,512]{1,0:T(8,128)(2,1)}, bf16[256,512]{1,0:T(8,128)(2,1)}) custom-call(bf16[256,512]{1,0:T(8,128)(2,1)} %get-tuple-element.5.linear, f32[4,256,128]{2,1,0:T(8,128)} %get-tuple-element.6.gated, f32[8,256]{1,0:T(8,128)} %get-tuple-element.7.total, f32[1,512]{1,0:T(1,128)} %bitcast.14), custom_call_target="tpu_custom_call" | custom-call | tf_op jit(solution)/shard_map/finish/pallas_call | solution.py:864
